TPU v7x, 128 devices: a whole 4x4x4 slice. The times are simulated.
128 devices in a mesh: kv: 32 (over z, y, core), tp: 4 (over x).
Axes of the slice: x: 4, y: 4, z: 4, core: 2. Of those that a mesh axis runs over, the one named last changes fastest.
Arguments:
- tokens: bfloat16 [16384, 2048], P('kv', 'tp'), may hold values from -9 to 9
- w_query: bfloat16 [2048, 1536], P(None, 'tp'), may hold values from -1 to 1
- w_key: bfloat16 [2048, 1536], P(None, 'tp'), may hold values from -1 to 1
- w_value: bfloat16 [2048, 1536], P(None, 'tp'), may hold values from -0.5 to 0.5
- w_out: bfloat16 [1536, 2048], P('tp'), may hold values from -0.15625 to 0.15625
- chosen: int32 [512, 24], P('kv'), may hold values from 0 to 511, as said below
Outputs:
- mixed: bfloat16 [16384, 2048], P(('kv', 'tp'))
Inputs may be any that keep to these rules, and one draw needn't show every extreme that they name: `chosen`: row c names blocks no later than c; its first entry is c and its second c - 1 (0 for row 0), and an entry may repeat. Taking the rows in aligned runs of 16, one run for each index of kv, the rows of one run name at most 2 distinct blocks lying in any one other index's positions; in every draw some index of kv names exactly 2 from every earlier index. Every run names some block of the index just before it and of the index half the axis before it, where those exist.
All inputs are finite; a program needn't handle non-finite values.
Results may differ from a plain program's by a relative error of at most 0.014.
Values may be sent and summed in bfloat16 or wider, within the bound.
No kernel may reach another device: no remote copies, remote signals or barrier semaphores. Data moves between devices by JAX's collectives and lax.ppermute only.
A program may use at most 320 MiB of HBM per device.

v0:
```python
import jax
import jax.numpy as jnp
from jax import lax
from jax.experimental import pallas as pl
from jax.experimental.pallas import tpu as pltpu
from jax.sharding import Mesh
from jax.sharding import PartitionSpec as P


HD = 128
BLK = 32
MOST = 2
KV = ("kv_0", "kv_1", "kv_2")
KV_TP = ("kv_0", "kv_1", "kv_2", "tp")
NEG = -1e30
LOG2E = 1.4426950408889634
SMALL = 24 * 1024 * 1024
LARGE = 60 * 1024 * 1024
HBM = pl.BlockSpec(memory_space=pltpu.HBM)
VMEM = pl.BlockSpec(memory_space=pltpu.VMEM)
SMEM = pl.BlockSpec(memory_space=pltpu.SMEM)


def params(limit=SMALL):
    return pltpu.CompilerParams(vmem_limit_bytes=limit)


def in_hbm(shape, dtype):
    return pltpu.HBM(shape, dtype)


def in_vmem(shape, dtype):
    return pltpu.VMEM(shape, dtype)


def cost(flops, nbytes, exps=0):
    return pl.CostEstimate(flops=int(flops), bytes_accessed=int(nbytes), transcendentals=int(exps))


def keep_in_hbm(*arrays):
    return tuple(pltpu.with_memory_space_constraint(a, pltpu.HBM) for a in arrays)


def f32dot(a, b):
    return jnp.dot(a, b, preferred_element_type=jnp.float32)


def shifted(array, axis, by):
    count = lax.axis_size(axis)
    return lax.ppermute(array, axis, [(i, (i + by) % count) for i in range(count)])


def project_near(where, own, left, right, w_key, w_value):
    rows, feat = own.shape
    width = w_key.shape[1]
    chunks = where.shape[0]

    def body(where_ref, own_hbm, l_ref, r_ref, wk_hbm, wv_hbm, tot_ref, wk_last, wv_last, l_hbm, r_hbm, *rest):
        own_ref, chunk_refs, sems = rest
        copies = []

        def fetch(src, dst):
            copies.append(pltpu.make_async_copy(src, dst, sems.at[len(copies)]))
            copies[-1].start()
            return copies[-1]

        own_copy = fetch(own_hbm, own_ref)
        pieces = []
        for k in range(chunks - 1):
            span = pl.ds(pl.multiple_of(where_ref[k] * feat, feat), feat)
            for j, w in enumerate((wk_hbm, wv_hbm)):
                pieces.append(fetch(w.at[span, :], chunk_refs.at[k, j]))
        span = pl.ds(pl.multiple_of(where_ref[chunks - 1] * feat, feat), feat)
        last = [fetch(wk_hbm.at[span, :], wk_last), fetch(wv_hbm.at[span, :], wv_last)]
        last += [fetch(l_ref, l_hbm), fetch(r_ref, r_hbm)]
        own_copy.wait()
        for copy in pieces:
            copy.wait()
        for j in range(2):
            total = f32dot(own_ref[...], chunk_refs[0, j]) + f32dot(l_ref[...], chunk_refs[1, j])
            tot_ref[:, j * width : (j + 1) * width] = total + f32dot(r_ref[...], chunk_refs[2, j])
        for copy in last:
            copy.wait()

    chunk = (feat, width)
    return pl.pallas_call(
        body,
        in_specs=[SMEM, HBM, VMEM, VMEM, HBM, HBM],
        out_specs=[VMEM, VMEM, VMEM, HBM, HBM],
        out_shape=[
            in_vmem((rows, 2 * width), jnp.float32),
            in_vmem(chunk, jnp.bfloat16),
            in_vmem(chunk, jnp.bfloat16),
            in_hbm((rows, feat), jnp.bfloat16),
            in_hbm((rows, feat), jnp.bfloat16),
        ],
        scratch_shapes=[
            pltpu.VMEM((rows, feat), jnp.bfloat16),
            pltpu.VMEM((chunks - 1, 2, feat, width), jnp.bfloat16),
            pltpu.SemaphoreType.DMA((2 * chunks + 3,)),
        ],
        compiler_params=params(),
        cost_estimate=cost(12 * rows * feat * width, 20 * feat * width),
        name="project_near",
    )(where, *keep_in_hbm(own), left, right, *keep_in_hbm(w_key, w_value))


def project_last(asked, top, bottom, wk_last, wv_last, total):
    half, feat = top.shape
    rows = 2 * half
    width = wk_last.shape[1]
    peers = asked.shape[0]
    slots = peers * MOST

    def body(asked_hbm, t_ref, b_ref, wk, wv, tot_ref, pair_hbm, send_hbm, t_hbm, b_hbm, pick, pair, sem, sems, sends):
        get = pltpu.make_async_copy(asked_hbm, pick, sem)
        get.start()
        keep = [
            pltpu.make_async_copy(t_ref, t_hbm, sems.at[0]),
            pltpu.make_async_copy(b_ref, b_hbm, sems.at[1]),
        ]
        for copy in keep:
            copy.start()
        for j, w in enumerate((wk, wv)):
            cols = slice(j * width, (j + 1) * width)
            for lo, ref in ((0, t_ref), (half, b_ref)):
                span = slice(lo, lo + half)
                pair[span, cols] = (tot_ref[span, cols] + f32dot(ref[...], w[...])).astype(jnp.bfloat16)
            if j == 0:
                get.wait()
            for i in range(slots):
                block = jnp.clip(pick[i // MOST, i % MOST], 0, rows // BLK - 1)
                span = pl.ds(pl.multiple_of(block * BLK, BLK), BLK)
                pltpu.make_async_copy(pair.at[span, cols], send_hbm.at[i, :, cols], sends.at[j]).start()
        copy = pltpu.make_async_copy(pair, pair_hbm, sems.at[2])
        copy.start()
        keep.append(copy)
        for copy in keep:
            copy.wait()
        for j in range(2):
            sent = send_hbm.at[:, :, j * width : (j + 1) * width]
            pltpu.make_async_copy(sent, sent, sends.at[j]).wait()

    return pl.pallas_call(
        body,
        in_specs=[HBM, VMEM, VMEM, VMEM, VMEM, VMEM],
        out_specs=[HBM, HBM, HBM, HBM],
        out_shape=[
            in_hbm((rows, 2 * width), jnp.bfloat16),
            in_hbm((slots, BLK, 2 * width), jnp.bfloat16),
            in_hbm((half, feat), jnp.bfloat16),
            in_hbm((half, feat), jnp.bfloat16),
        ],
        scratch_shapes=[
            pltpu.SMEM((peers, HD), jnp.int32),
            pltpu.VMEM((rows, 2 * width), jnp.bfloat16),
            pltpu.SemaphoreType.DMA,
            pltpu.SemaphoreType.DMA((3,)),
            pltpu.SemaphoreType.DMA((2,)),
        ],
        compiler_params=params(),
        cost_estimate=cost(4 * rows * feat * width, 12 * feat * width),
        name="project_last",
    )(asked, top, bottom, wk_last, wv_last, total)


def project_query(where, own, left, right, top, bottom, w_query):
    rows, feat = own.shape
    half = top.shape[0]
    width = w_query.shape[1]

    def body(where_ref, o_ref, l_ref, r_ref, t_ref, b_ref, wo, wl, wr, wf, out_ref):
        for lo, far in ((0, t_ref), (half, b_ref)):
            span = slice(lo, lo + half)
            total = f32dot(o_ref[span, :], wo[...]) + f32dot(l_ref[span, :], wl[...])
            total = total + f32dot(r_ref[span, :], wr[...]) + f32dot(far[...], wf[...])
            out_ref[span, :] = total.astype(jnp.bfloat16)

    def chunk(k):
        return pl.BlockSpec((feat, width), lambda i, s: (s[k], 0))

    toks = pl.BlockSpec((rows, feat), lambda i, s: (0, 0))
    halves = pl.BlockSpec((half, feat), lambda i, s: (0, 0))
    return pl.pallas_call(
        body,
        grid_spec=pltpu.PrefetchScalarGridSpec(
            num_scalar_prefetch=1,
            grid=(1,),
            in_specs=[toks, toks, toks, halves, halves, chunk(0), chunk(1), chunk(2), chunk(3)],
            out_specs=pl.BlockSpec((rows, width), lambda i, s: (0, 0)),
        ),
        out_shape=in_hbm((rows, width), jnp.bfloat16),
        compiler_params=params(LARGE),
        cost_estimate=cost(8 * rows * feat * width, 16 * feat * width),
        name="project_query",
    )(where, *keep_in_hbm(own, left, right, top, bottom, w_query, w_query, w_query, w_query))


def plan(my_index, chosen, peers):
    rows, wide = chosen.shape
    slots = peers * MOST

    def body(me_ref, cho_ref, req_ref, mask_ref):
        me = me_ref[0]
        entries = cho_ref[...]
        peer = lax.broadcasted_iota(jnp.int32, (peers, wide), 0)
        low = jnp.full((peers, wide), rows, jnp.int32)
        high = jnp.full((peers, wide), -1, jnp.int32)
        for r in range(rows):
            entry = jnp.broadcast_to(entries[r : r + 1, :], (peers, wide))
            block = entry - peer * rows
            mine = (block >= 0) & (block < rows)
            low = jnp.where(mine, jnp.minimum(low, block), low)
            high = jnp.where(mine, jnp.maximum(high, block), high)
        low = jnp.min(low, axis=1, keepdims=True)
        high = jnp.max(high, axis=1, keepdims=True)
        far = lax.broadcasted_iota(jnp.int32, (peers, 1), 0) != me
        first = jnp.where(far & (low < rows), low, -1)
        second = jnp.where(far & (high > low), high, -1)
        lane = lax.broadcasted_iota(jnp.int32, (peers, HD), 1)
        req_ref[...] = jnp.where(lane == 0, first, jnp.where(lane == 1, second, -1))
        at = lax.broadcasted_iota(jnp.int32, (peers, HD), 0)
        named = jnp.where(lane == MOST * at, first, jnp.where(lane == MOST * at + 1, second, -1))
        named = jnp.where(named >= 0, named + at * rows, -1)
        ids = jnp.max(named, axis=0, keepdims=True)
        slot = lax.broadcasted_iota(jnp.int32, (1, HD), 1)
        own = (slot >= slots) & (slot < slots + rows)
        ids = jnp.where(own, me * rows + slot - slots, ids)
        seen = entries[:, :1] == ids
        for k in range(1, wide):
            seen = seen | (entries[:, k : k + 1] == ids)
        bias = jnp.where(seen, 0.0, NEG)
        for r in range(rows):
            mask_ref[r * BLK : (r + 1) * BLK, :] = jnp.broadcast_to(bias[r : r + 1, :], (BLK, HD)).astype(jnp.bfloat16)

    return pl.pallas_call(
        body,
        grid_spec=pltpu.PrefetchScalarGridSpec(
            num_scalar_prefetch=1,
            grid=(1,),
            in_specs=[pl.BlockSpec((rows, wide), lambda i, s: (0, 0))],
            out_specs=[
                pl.BlockSpec((peers, HD), lambda i, s: (0, 0)),
                pl.BlockSpec((rows * BLK, HD), lambda i, s: (0, 0)),
            ],
        ),
        out_shape=[in_hbm((peers, HD), jnp.int32), in_hbm((rows * BLK, HD), jnp.bfloat16)],
        compiler_params=params(),
        cost_estimate=cost(1000000, 200000),
        name="plan",
    )(my_index, chosen)


def one_hot(rows, first_slot):
    slot = lax.broadcasted_iota(jnp.int32, (rows, HD), 0) // BLK + first_slot
    return (slot == lax.broadcasted_iota(jnp.int32, (rows, HD), 1)).astype(jnp.bfloat16)


def scores_of(query, keys):
    return lax.dot_general(query, keys, (((1,), (1,)), ((), ())), preferred_element_type=jnp.float32)


def attend_own(query, pair, mask, first_slot):
    rows, width = query.shape
    heads = width // HD
    scale = HD ** (-0.5) * LOG2E
    tile = 256

    def body(q_ref, k_ref, v_ref, mask_ref, high_ref, tot_ref, sum_ref):
        keys = jnp.concatenate([k_ref[...], one_hot(rows, first_slot)], axis=1)
        values = jnp.concatenate([v_ref[...], jnp.ones_like(v_ref)], axis=1)
        for lo in range(0, rows, tile):
            span = slice(lo, lo + tile)
            count = lo + tile
            wide = jnp.concatenate([q_ref[span, :], mask_ref[span, :]], axis=1)
            scores = scores_of(wide, keys[:count])
            row = lax.broadcasted_iota(jnp.int32, scores.shape, 0) + lo
            col = lax.broadcasted_iota(jnp.int32, scores.shape, 1)
            scores = jnp.where(col <= row, scores, NEG)
            high = jnp.max(scores, axis=1, keepdims=True)
            weights = jnp.exp2((scores - high) * scale).astype(jnp.bfloat16)
            summed = f32dot(weights, values[:count])
            high_ref[span, :] = jnp.broadcast_to(high, (tile, HD))
            tot_ref[span, :] = summed[:, HD:]
            sum_ref[span, :] = summed[:, :HD]

    column = pl.BlockSpec((rows, HD), lambda h: (0, h))
    return pl.pallas_call(
        body,
        grid=(heads,),
        in_specs=[
            column,
            column,
            pl.BlockSpec((rows, HD), lambda h: (0, heads + h)),
            pl.BlockSpec((rows, HD), lambda h: (0, 0)),
        ],
        out_specs=[column, column, column],
        out_shape=[in_hbm((rows, width), jnp.float32)] * 3,
        compiler_params=params(LARGE),
        cost_estimate=cost(8 * rows * rows * width, 16 * rows * width, rows * rows * heads),
        name="attend_own",
    )(query, pair, pair, mask)


def attend_far(where, query, got, mask, high, total, summed, carried):
    rows, width = query.shape
    heads = width // HD
    count = got.shape[0]
    scale = HD ** (-0.5) * LOG2E
    parts = where.shape[0]
    tile = rows // parts
    pairs = ((3, 1), (2, 0))

    def body(where_ref, q_ref, k_ref, v_ref, mask_ref, high_ref, tot_ref, sum_ref, *rest):
        pieces = len(carried)
        copies = [
            pltpu.make_async_copy(rest[k], rest[pieces + parts + k], rest[-1].at[k]) for k in range(pieces)
        ]
        outs = rest[pieces : pieces + parts]
        keys, values = rest[-3:-1]

        @pl.when(pl.program_id(0) == 1)
        def _():
            for copy in copies:
                copy.start()

        @pl.when(pl.program_id(0) == 0)
        def _():
            keys[:, HD:] = one_hot(count, 0)
            values[:, HD:] = jnp.ones_like(v_ref)

        keys[:, :HD] = k_ref[...]
        values[:, :HD] = v_ref[...]

        def rows_of(ref, parts_at):
            spans = [pl.ds(pl.multiple_of(where_ref[p] * tile, tile), tile) for p in parts_at]
            return jnp.concatenate([ref[span, :] for span in spans], axis=0)

        def scores_at(parts_at):
            wide = jnp.concatenate([rows_of(q_ref, parts_at), rows_of(mask_ref, parts_at)], axis=1)
            return scores_of(wide, keys[...])

        later = scores_at(pairs[0])
        for i, parts_at in enumerate(pairs):
            scores = later
            if i + 1 < len(pairs):
                later = scores_at(pairs[i + 1])
            own = rows_of(high_ref, parts_at)
            top = jnp.maximum(jnp.max(scores, axis=1, keepdims=True), own[:, :1])
            weights = jnp.exp2((scores - top) * scale).astype(jnp.bfloat16)
            far = f32dot(weights, values[...])
            keep = jnp.exp2((own - top) * scale)
            result = far[:, :HD] + keep * rows_of(sum_ref, parts_at)
            result = (result / (far[:, HD:] + keep * rows_of(tot_ref, parts_at))).astype(jnp.bfloat16)
            for k, part in enumerate(parts_at):
                outs[part][...] = result[k * tile : (k + 1) * tile]

        @pl.when(pl.program_id(0) == heads - 1)
        def _():
            for copy in copies:
                copy.wait()

    column = pl.BlockSpec((rows, HD), lambda h, s: (0, h))
    return pl.pallas_call(
        body,
        grid_spec=pltpu.PrefetchScalarGridSpec(
            num_scalar_prefetch=1,
            grid=(heads,),
            in_specs=[
                column,
                pl.BlockSpec((count, HD), lambda h, s: (0, h)),
                pl.BlockSpec((count, HD), lambda h, s: (0, heads + h)),
                pl.BlockSpec((rows, HD), lambda h, s: (0, 0)),
                column,
                column,
                column,
            ]
            + [HBM] * len(carried),
            out_specs=[pl.BlockSpec((tile, HD), lambda h, s: (0, h))] * parts + [VMEM] * len(carried),
            scratch_shapes=[pltpu.VMEM((count, 2 * HD), jnp.bfloat16)] * 2
            + [pltpu.SemaphoreType.DMA((len(carried),))],
        ),
        out_shape=[jax.ShapeDtypeStruct((tile, width), jnp.bfloat16)] * parts
        + [in_vmem(w.shape, w.dtype) for w in carried],
        compiler_params=params(),
        cost_estimate=cost(8 * rows * count * width, 4 * count * width, rows * count * heads),
        name="attend_far",
    )(where, *keep_in_hbm(query), got, got, *keep_in_hbm(mask, high, total, summed, *carried))


def mix(core, attended, w_own, mine, other):
    rows, width = attended[0].shape
    span = mine[0].shape[1]
    part = mine[2].shape[1]

    def body(core_ref, own_ref, l_ref, r_ref, f_ref, w_ref, *rest):
        out_hbm, out_ref, sems = rest[8:]
        copies = []
        for side, pieces in enumerate((rest[:4], rest[4:8])):
            at = pl.multiple_of((core_ref[0] if side == 0 else 1 - core_ref[0]) * span, span)
            total = f32dot(own_ref[...], w_ref[:, pl.ds(at, span)])
            total = total + f32dot(l_ref[...], pieces[0][...]) + f32dot(r_ref[...], pieces[1][...])
            for k in range(2):
                to = slice(k * part, (k + 1) * part)
                value = total[:, to] + f32dot(f_ref[...], pieces[2 + k][...])
                out_ref[side, :, to] = value.astype(jnp.bfloat16)
            copies.append(pltpu.make_async_copy(out_ref.at[side], out_hbm.at[:, pl.ds(at, span)], sems.at[side]))
            copies[-1].start()
        for copy in copies:
            copy.wait()

    args = (*attended, w_own, *mine, *other)
    return pl.pallas_call(
        body,
        in_specs=[SMEM] + [VMEM] * len(args),
        out_specs=HBM,
        out_shape=in_hbm((rows, 2 * span), jnp.bfloat16),
        scratch_shapes=[pltpu.VMEM((2, rows, span), jnp.bfloat16), pltpu.SemaphoreType.DMA((2,))],
        compiler_params=params(),
        cost_estimate=cost(16 * rows * width * span, 16 * width * span),
        name="mix",
    )(core, *args)


def local(tokens, w_query, w_key, w_value, w_out, chosen):
    tok_rows = tokens.shape[0]
    width = w_query.shape[1]
    half = tok_rows // 2
    peers = lax.axis_size(KV)
    tp = lax.axis_index("tp")
    count = lax.axis_size("tp")
    where = jnp.stack([tp, (tp + count - 1) % count, (tp + 1) % count, (tp + 2) % count]).astype(jnp.int32)
    me = jnp.reshape(lax.axis_index(KV), (1,)).astype(jnp.int32)
    core = jnp.reshape(lax.axis_index("kv_2"), (1,)).astype(jnp.int32)
    tokens, where, me, core = lax.optimization_barrier((tokens, where, me, core))

    left = shifted(tokens, "tp", 1)
    right = shifted(tokens, "tp", -1)
    request, mask = plan(me, chosen, peers)
    asked = lax.all_to_all(request, KV, 0, 0, tiled=True)
    left, right, request, mask = lax.optimization_barrier((left, right, request, mask))

    top = shifted(left[:half], "tp", 1)
    bottom = shifted(right[half:], "tp", -1)
    total, wk_last, wv_last, left, right = project_near(where, tokens, left, right, w_key, w_value)
    pair, send, top, bottom = project_last(asked, top, bottom, wk_last, wv_last, total)
    w_mine, send = lax.optimization_barrier((w_out, send))
    got = lax.all_to_all(send, KV, split_axis=0, concat_axis=0, tiled=True)

    span = w_out.shape[1] // 2
    part = span // 2
    piece = lax.dynamic_slice_in_dim(w_mine, core[0] * span, span, axis=1)
    w_left = shifted(piece, "tp", 1)
    w_right = shifted(piece, "tp", -1)
    w_low = shifted(w_left[:, :part], "tp", 1)
    w_high = shifted(w_right[:, part:], "tp", -1)
    mine = (w_left, w_right, w_low, w_high)
    other = tuple(shifted(w, "kv_2", 1) for w in mine)

    query = project_query(where, tokens, left, right, top, bottom, w_query)
    high, totals, summed = attend_own(query, pair, mask, peers * MOST)
    weights = (w_out, *mine, *other)
    outs = attend_far(where, query, got.reshape(-1, 2 * width), mask, high, totals, summed, weights)
    attended = (outs[0], shifted(outs[2], "tp", 1), shifted(outs[1], "tp", -1), shifted(outs[3], "tp", 2))
    return mix(core, attended, outs[4], outs[5:9], outs[9:])


def solution(mesh):
    finer = Mesh(mesh.devices.reshape(4, 4, 2, mesh.shape["tp"]), ("kv_0", "kv_1", "kv_2", "tp"))
    placed = (P(KV, "tp"), P(None, "tp"), P(None, "tp"), P(None, "tp"), P("tp", None), P(KV, None))

    return jax.shard_map(local, mesh=finer, in_specs=placed, out_specs=P(KV_TP, None), check_vma=False)
```

profile of v0, /device:TPU:0, one launch (start us, length us, event | category | flops | bytes accessed | tf_op | source)
XLA Modules:
  0.0 112.8 jit_solution(18200185462110216082)
XLA Ops:
  0.1 2.9 %collective-permute-start.1 = (bf16[512,512]{1,0:T(8,128)(2,1)}, bf16[512,512]{1,0:T(8,128)(2,1)S(1)}, u32[]{:S(2)}, u32[]{:S(2)}) collective-permute-start(bf16[512,512]{1,0:T(8,128)(2,1)} %o_ref), channel_id=1, source_target_pairs={{0,3},{1,0},{2,1},{3,2},{4,7},{5,4},{6,5},{7,6},{8,11},{9,8},{10,9... | collective-permute-start | bytes 1572872 | tf_op jit(solution)/shard_map/ppermute | solution.py:50
  3.0 0.7 copy-done.2
  3.7 1.0 plan.1
  4.6 9.8 %collective-permute-done.1.r_ref = bf16[512,512]{1,0:T(8,128)(2,1)S(1)} collective-permute-done((bf16[512,512]{1,0:T(8,128)(2,1)}, bf16[512,512]{1,0:T(8,128)(2,1)S(1)}, u32[]{:S(2)}, u32[]{:S(2)}) %collective-permute-start.1) | collective-permute-done | bytes 524320 | tf_op jit(solution)/shard_map/ppermute | solution.py:50
  14.5 3.3 %collective-permute-done.l_ref = bf16[512,512]{1,0:T(8,128)(2,1)S(1)} collective-permute-done((bf16[512,512]{1,0:T(8,128)(2,1)}, bf16[512,512]{1,0:T(8,128)(2,1)S(1)}, u32[]{:S(2)}, u32[]{:S(2)}) %collective-permute-start) | collective-permute-done | bytes 524320 | tf_op jit(solution)/shard_map/ppermute | solution.py:50
  17.8 0.7 slice.12
  18.5 0.7 slice.13
  19.2 0.3 collective-permute-start.3
  19.5 1.7 %collective-permute-start.2 = (bf16[256,512]{1,0:T(8,128)(2,1)}, bf16[256,512]{1,0:T(8,128)(2,1)}, u32[]{:S(2)}, u32[]{:S(2)}) collective-permute-start(bf16[256,512]{1,0:T(8,128)(2,1)} %slice.12), channel_id=1, source_target_pairs={{0,1},{1,2},{2,3},{3,0},{4,5},{5,6},{6,7},{7,4},{8,9},{9,10},{10,1... | collective-permute-start | bytes 786440 | tf_op jit(solution)/shard_map/ppermute | solution.py:50
  21.3 8.3 %all-to-all-start = ((s32[32,1,128]{2,1,0:T(1,128)}), s32[32,1,128]{2,1,0:T(1,128)S(1)}, u32[]{:S(2)}, u32[]{:S(2)}) async-start(s32[32,1,128]{2,1,0:T(1,128)} %bitcast.15), calls=%async_computation | async-start | bytes 32768 | tf_op jit(solution)/shard_map/all_to_all | solution.py:440
  29.6 4.6 %project_near.1 = (f32[512,768]{1,0:T(8,128)S(1)}, bf16[512,384]{1,0:T(8,128)(2,1)S(1)}, bf16[512,384]{1,0:T(8,128)(2,1)S(1)}, bf16[512,512]{1,0:T(8,128)(2,1)}, bf16[512,512]{1,0:T(8,128)(2,1)}) custom-call(s32[4]{0:T(128)S(1)} %pad_add_fusion.where_ref, bf16[512,512]{1,0:T(8,128)(2,1)} %o_ref, bf16[512,512]{1,0:T(8,128)(2,1)S(1)} %collective-permute-done.l_ref, ...), custom_call_target="tpu_custom_call" | custom-call | flops 1207959552 | bytes 3932160 | tf_op jit(solution)/shard_map/project_near/pallas_call | solution.py:86
  34.2 2.8 %all-to-all-done = s32[32,1,128]{2,1,0:T(1,128)S(1)} async-done(((s32[32,1,128]{2,1,0:T(1,128)}), s32[32,1,128]{2,1,0:T(1,128)S(1)}, u32[]{:S(2)}, u32[]{:S(2)}) %all-to-all-start) | async-done | bytes 16416 | tf_op jit(solution)/shard_map/all_to_all | solution.py:440
  37.0 3.8 %project_last.1 = (bf16[512,768]{1,0:T(8,128)(2,1)}, bf16[64,32,768]{2,1,0:T(8,128)(2,1)}, bf16[256,512]{1,0:T(8,128)(2,1)}, bf16[256,512]{1,0:T(8,128)(2,1)}) custom-call(s32[32,128]{1,0:T(8,128)S(1)} %bitcast.14, bf16[256,512]{1,0:T(8,128)(2,1)} %collective-permute-done.2.t_ref, bf16[256,512]{1,0:T(8,128)(2,1)} %collective-permute-done.3.b_ref, ...), custom_call_target="tpu_custom_call" | custom-call | flops 402653184 | bytes 2359296 | tf_op jit(solution)/shard_map/project_last/pallas_call | solution.py:144
  40.8 4.6 %all-to-all-start.1 = ((bf16[64,32,768]{2,1,0:T(8,128)(2,1)}), bf16[64,32,768]{2,1,0:T(8,128)(2,1)S(1)}, u32[]{:S(2)}, u32[]{:S(2)}) async-start(bf16[64,32,768]{2,1,0:T(8,128)(2,1)} %get-tuple-element.57), calls=%async_computation.1 | async-start | bytes 6291456 | tf_op jit(solution)/shard_map/all_to_all | solution.py:448
  45.5 1.2 %constant_dynamic-slice_fusion = bf16[384,1024]{1,0:T(8,128)(2,1)S(1)} fusion(bf16[384,2048]{1,0:T(8,128)(2,1)} %rest_0_.1, s32[]{:T(128)S(6)} %select_n.21), kind=kLoop, calls=%fused_computation.1 | loop fusion | bytes 1572868 | tf_op jit(solution)/shard_map/dynamic_slice | solution.py:452
  46.6 1.6 %collective-permute-start.5 = (bf16[384,1024]{1,0:T(8,128)(2,1)S(1)}, bf16[384,1024]{1,0:T(8,128)(2,1)}, u32[]{:S(2)}, u32[]{:S(2)}) collective-permute-start(bf16[384,1024]{1,0:T(8,128)(2,1)S(1)} %constant_dynamic-slice_fusion), channel_id=1, source_target_pairs={{0,3},{1,0},{2,1},{3,2},{4,7},{5,4},{6,5},{7,6},{8,11},{9,8},{10,9... | collective-permute-start | bytes 2359304 | tf_op jit(solution)/shard_map/ppermute | solution.py:50
  48.2 0.5 collective-permute-start.4
  48.7 17.8 %collective-permute-done.5.rest_2_ = bf16[384,1024]{1,0:T(8,128)(2,1)} collective-permute-done((bf16[384,1024]{1,0:T(8,128)(2,1)S(1)}, bf16[384,1024]{1,0:T(8,128)(2,1)}, u32[]{:S(2)}, u32[]{:S(2)}) %collective-permute-start.5) | collective-permute-done | bytes 786464 | tf_op jit(solution)/shard_map/ppermute | solution.py:50
  66.5 1.0 slice.17
  67.6 2.8 %collective-permute-start.7 = (bf16[384,512]{1,0:T(8,128)(2,1)S(1)}, bf16[384,512]{1,0:T(8,128)(2,1)S(1)}, u32[]{:S(2)}, u32[]{:S(2)}) collective-permute-start(bf16[384,512]{1,0:T(8,128)(2,1)S(1)} %slice.17), channel_id=1, source_target_pairs={{0,3},{1,0},{2,1},{3,2},{4,7},{5,4},{6,5},{7,6},{8,11},{9,8},{10,9... | collective-permute-start | bytes 1179656 | tf_op jit(solution)/shard_map/ppermute | solution.py:50
  70.3 1.0 slice.16
  71.5 0.6 collective-permute-start.8
  72.0 6.3 %collective-permute-done.7.rest_4_ = bf16[384,512]{1,0:T(8,128)(2,1)S(1)} collective-permute-done((bf16[384,512]{1,0:T(8,128)(2,1)S(1)}, bf16[384,512]{1,0:T(8,128)(2,1)S(1)}, u32[]{:S(2)}, u32[]{:S(2)}) %collective-permute-start.7) | collective-permute-done | bytes 393248 | tf_op jit(solution)/shard_map/ppermute | solution.py:50
  78.3 5.9 %collective-permute-done.6.rest_3_ = bf16[384,512]{1,0:T(8,128)(2,1)S(1)} collective-permute-done((bf16[384,512]{1,0:T(8,128)(2,1)S(1)}, bf16[384,512]{1,0:T(8,128)(2,1)S(1)}, u32[]{:S(2)}, u32[]{:S(2)}) %collective-permute-start.6) | collective-permute-done | bytes 393248 | tf_op jit(solution)/shard_map/ppermute | solution.py:50
  84.2 4.6 %project_query.1.q_ref = bf16[512,384]{1,0:T(8,128)(2,1)} custom-call(s32[4]{0:T(128)} %copy-done, bf16[512,512]{1,0:T(8,128)(2,1)} %o_ref, bf16[512,512]{1,0:T(8,128)(2,1)} %get-tuple-element.49.l_ref, bf16[512,512]{1,0:T(8,128)(2,1)} %get-tuple-element.50.r_ref, bf16[256,512]{1,0:T(8,128)(2,1)} %get-tuple-element.54.t_ref, ...), custom_call_target="tpu_custom_call" | custom-call | flops 805306368 | bytes 3145728 | tf_op jit(solution)/shard_map/project_query/pallas_call | solution.py:184
  88.8 4.9 %attend_own.1 = (f32[512,384]{1,0:T(8,128)}, f32[512,384]{1,0:T(8,128)}, f32[512,384]{1,0:T(8,128)}) custom-call(bf16[512,384]{1,0:T(8,128)(2,1)} %project_query.1.q_ref, bf16[512,768]{1,0:T(8,128)(2,1)} %get-tuple-element.59.k_ref.v_ref, bf16[512,768]{1,0:T(8,128)(2,1)} %get-tuple-element.59.k_ref.v_ref, bf16[512,128]{1,0:T(8,128)(2,1)} %get-tuple-element.58.mask_ref), custom_call_target="tpu_custom_call" | custom-call | flops 805306368 | bytes 3145728 | tf_op jit(solution)/shard_map/attend_own/pallas_call | solution.py:288
  93.8 7.5 %attend_far.1 = (bf16[128,384]{1,0:T(8,128)(2,1)S(1)}, bf16[128,384]{1,0:T(8,128)(2,1)S(1)}, bf16[128,384]{1,0:T(8,128)(2,1)S(1)}, bf16[128,384]{1,0:T(8,128)(2,...) custom-call(s32[4]{0:T(128)S(1)} %copy-done.1, ...), custom_call_target="tpu_custom_call" | custom-call | flops 3221225472 | bytes 3145728 | tf_op jit(solution)/shard_map/attend_far/pallas_call | solution.py:364
  101.5 3.2 %collective-permute-start.13 = (bf16[128,384]{1,0:T(8,128)(2,1)S(1)}, bf16[128,384]{1,0:T(8,128)(2,1)S(1)}, u32[]{:S(2)}, u32[]{:S(2)}) collective-permute-start(bf16[128,384]{1,0:T(8,128)(2,1)S(1)} %get-tuple-element.66), channel_id=1, source_target_pairs={{0,3},{1,0},{2,1},{3,2},{4,7},{5,4},{6,5},{7,6},{8,11},{9,8},{10,9... | collective-permute-start | bytes 294920 | tf_op jit(solution)/shard_map/ppermute | solution.py:50
  104.7 3.2 %collective-permute-done.12.l_ref = bf16[128,384]{1,0:T(8,128)(2,1)S(1)} collective-permute-done((bf16[128,384]{1,0:T(8,128)(2,1)S(1)}, bf16[128,384]{1,0:T(8,128)(2,1)S(1)}, u32[]{:S(2)}, u32[]{:S(2)}) %collective-permute-start.12) | collective-permute-done | bytes 98336 | tf_op jit(solution)/shard_map/ppermute | solution.py:50
  107.9 1.4 %collective-permute-done.13.r_ref = bf16[128,384]{1,0:T(8,128)(2,1)S(1)} collective-permute-done((bf16[128,384]{1,0:T(8,128)(2,1)S(1)}, bf16[128,384]{1,0:T(8,128)(2,1)S(1)}, u32[]{:S(2)}, u32[]{:S(2)}) %collective-permute-start.13) | collective-permute-done | bytes 98336 | tf_op jit(solution)/shard_map/ppermute | solution.py:50
  109.3 1.6 %collective-permute-done.14.f_ref = bf16[128,384]{1,0:T(8,128)(2,1)S(1)} collective-permute-done((bf16[128,384]{1,0:T(8,128)(2,1)S(1)}, bf16[128,384]{1,0:T(8,128)(2,1)S(1)}, u32[]{:S(2)}, u32[]{:S(2)}) %collective-permute-start.14) | collective-permute-done | bytes 98336 | tf_op jit(solution)/shard_map/ppermute | solution.py:50
  110.9 2.0 %mix.1 = bf16[128,2048]{1,0:T(8,128)(2,1)} custom-call(s32[1]{0:T(128)} %bitcast.5.core_ref, bf16[128,384]{1,0:T(8,128)(2,1)S(1)} %get-tuple-element.64.own_ref, bf16[128,384]{1,0:T(8,128)(2,1)S(1)} %collective-permute-done.12.l_ref, bf16[128,384]{1,0:T(8,128)(2,1)S(1)} %collective-permute-done.13.r_ref, bf16[128,384]{1,0:T(8,128)(2,1)S(1)} %collective-permute-done.14.f_ref, ...), custom_call_target="tpu_custom_call" | custom-call | flops 805306368 | bytes 6291456 | tf_op jit(solution)/shard_map/mix/pallas_call | solution.py:413
  (25 shorter events, 0.3 us)
Async XLA Ops:
  0.1 34.1 %copy-start = (s32[4]{0:T(128)}, s32[4]{0:T(128)S(1)}, u32[]{:S(2)}) copy-start(s32[4]{0:T(128)S(1)} %pad_add_fusion.where_ref) | copy-start | bytes 52
  0.1 14.4 %collective-permute-start.1 = (bf16[512,512]{1,0:T(8,128)(2,1)}, bf16[512,512]{1,0:T(8,128)(2,1)S(1)}, u32[]{:S(2)}, u32[]{:S(2)}) collective-permute-start(bf16[512,512]{1,0:T(8,128)(2,1)} %o_ref), channel_id=1, source_target_pairs={{0,3},{1,0},{2,1},{3,2},{4,7},{5,4},{6,5},{7,6},{8,11},{9,8},{10,9... | collective-permute-start | bytes 1572872 | tf_op jit(solution)/shard_map/ppermute | solution.py:50
  3.0 14.8 %collective-permute-start = (bf16[512,512]{1,0:T(8,128)(2,1)}, bf16[512,512]{1,0:T(8,128)(2,1)S(1)}, u32[]{:S(2)}, u32[]{:S(2)}) collective-permute-start(bf16[512,512]{1,0:T(8,128)(2,1)} %o_ref), channel_id=1, source_target_pairs={{0,1},{1,2},{2,3},{3,0},{4,5},{5,6},{6,7},{7,4},{8,9},{9,10},{10,1... | collective-permute-start | bytes 1572872 | tf_op jit(solution)/shard_map/ppermute | solution.py:50
  3.0 0.7 copy-start.2
  19.2 17.8 %collective-permute-start.3 = (bf16[256,512]{1,0:T(8,128)(2,1)}, bf16[256,512]{1,0:T(8,128)(2,1)}, u32[]{:S(2)}, u32[]{:S(2)}) collective-permute-start(bf16[256,512]{1,0:T(8,128)(2,1)} %slice.13), channel_id=1, source_target_pairs={{0,3},{1,0},{2,1},{3,2},{4,7},{5,4},{6,5},{7,6},{8,11},{9,8},{10,9... | collective-permute-start | bytes 786440 | tf_op jit(solution)/shard_map/ppermute | solution.py:50
  19.5 17.5 %collective-permute-start.2 = (bf16[256,512]{1,0:T(8,128)(2,1)}, bf16[256,512]{1,0:T(8,128)(2,1)}, u32[]{:S(2)}, u32[]{:S(2)}) collective-permute-start(bf16[256,512]{1,0:T(8,128)(2,1)} %slice.12), channel_id=1, source_target_pairs={{0,1},{1,2},{2,3},{3,0},{4,5},{5,6},{6,7},{7,4},{8,9},{9,10},{10,1... | collective-permute-start | bytes 786440 | tf_op jit(solution)/shard_map/ppermute | solution.py:50
  21.3 15.7 %all-to-all-start = ((s32[32,1,128]{2,1,0:T(1,128)}), s32[32,1,128]{2,1,0:T(1,128)S(1)}, u32[]{:S(2)}, u32[]{:S(2)}) async-start(s32[32,1,128]{2,1,0:T(1,128)} %bitcast.15), calls=%async_computation | async-start | bytes 32768 | tf_op jit(solution)/shard_map/all_to_all | solution.py:440
  40.8 53.0 %all-to-all-start.1 = ((bf16[64,32,768]{2,1,0:T(8,128)(2,1)}), bf16[64,32,768]{2,1,0:T(8,128)(2,1)S(1)}, u32[]{:S(2)}, u32[]{:S(2)}) async-start(bf16[64,32,768]{2,1,0:T(8,128)(2,1)} %get-tuple-element.57), calls=%async_computation.1 | async-start | bytes 6291456 | tf_op jit(solution)/shard_map/all_to_all | solution.py:448
  46.6 19.9 %collective-permute-start.5 = (bf16[384,1024]{1,0:T(8,128)(2,1)S(1)}, bf16[384,1024]{1,0:T(8,128)(2,1)}, u32[]{:S(2)}, u32[]{:S(2)}) collective-permute-start(bf16[384,1024]{1,0:T(8,128)(2,1)S(1)} %constant_dynamic-slice_fusion), channel_id=1, source_target_pairs={{0,3},{1,0},{2,1},{3,2},{4,7},{5,4},{6,5},{7,6},{8,11},{9,8},{10,9... | collective-permute-start | bytes 2359304 | tf_op jit(solution)/shard_map/ppermute | solution.py:50
  48.2 22.1 %collective-permute-start.4 = (bf16[384,1024]{1,0:T(8,128)(2,1)S(1)}, bf16[384,1024]{1,0:T(8,128)(2,1)}, u32[]{:S(2)}, u32[]{:S(2)}) collective-permute-start(bf16[384,1024]{1,0:T(8,128)(2,1)S(1)} %constant_dynamic-slice_fusion), channel_id=1, source_target_pairs={{0,1},{1,2},{2,3},{3,0},{4,5},{5,6},{6,7},{7,4},{8,9},{9,10},{10,1... | collective-permute-start | bytes 2359304 | tf_op jit(solution)/shard_map/ppermute | solution.py:50
  67.6 10.7 %collective-permute-start.7 = (bf16[384,512]{1,0:T(8,128)(2,1)S(1)}, bf16[384,512]{1,0:T(8,128)(2,1)S(1)}, u32[]{:S(2)}, u32[]{:S(2)}) collective-permute-start(bf16[384,512]{1,0:T(8,128)(2,1)S(1)} %slice.17), channel_id=1, source_target_pairs={{0,3},{1,0},{2,1},{3,2},{4,7},{5,4},{6,5},{7,6},{8,11},{9,8},{10,9... | collective-permute-start | bytes 1179656 | tf_op jit(solution)/shard_map/ppermute | solution.py:50
  70.3 23.5 %collective-permute-start.9 = (bf16[384,1024]{1,0:T(8,128)(2,1)}, bf16[384,1024]{1,0:T(8,128)(2,1)}, u32[]{:S(2)}, u32[]{:S(2)}) collective-permute-start(bf16[384,1024]{1,0:T(8,128)(2,1)} %collective-permute-done.5.rest_2_), channel_id=1, source_target_pairs={{0,4},{4,0},{1,5},{5,1},{2,6},{6,2},{3,7},{7,3},{8,12},{12,8},{9,1... | collective-permute-start | bytes 2359304 | tf_op jit(solution)/shard_map/ppermute | solution.py:50
  71.4 12.8 %collective-permute-start.6 = (bf16[384,512]{1,0:T(8,128)(2,1)S(1)}, bf16[384,512]{1,0:T(8,128)(2,1)S(1)}, u32[]{:S(2)}, u32[]{:S(2)}) collective-permute-start(bf16[384,512]{1,0:T(8,128)(2,1)S(1)} %slice.16), channel_id=1, source_target_pairs={{0,1},{1,2},{2,3},{3,0},{4,5},{5,6},{6,7},{7,4},{8,9},{9,10},{10,1... | collective-permute-start | bytes 1179656 | tf_op jit(solution)/shard_map/ppermute | solution.py:50
  71.5 22.4 %collective-permute-start.8 = (bf16[384,1024]{1,0:T(8,128)(2,1)}, bf16[384,1024]{1,0:T(8,128)(2,1)}, u32[]{:S(2)}, u32[]{:S(2)}) collective-permute-start(bf16[384,1024]{1,0:T(8,128)(2,1)} %collective-permute-done.4.rest_1_), channel_id=1, source_target_pairs={{0,4},{4,0},{1,5},{5,1},{2,6},{6,2},{3,7},{7,3},{8,12},{12,8},{9,1... | collective-permute-start | bytes 2359304 | tf_op jit(solution)/shard_map/ppermute | solution.py:50
  78.3 10.5 %copy-start.3 = (bf16[384,512]{1,0:T(8,128)(2,1)}, bf16[384,512]{1,0:T(8,128)(2,1)S(1)}, u32[]{:S(2)}) copy-start(bf16[384,512]{1,0:T(8,128)(2,1)S(1)} %collective-permute-done.7.rest_4_) | copy-start | bytes 1179652
  78.3 15.5 %collective-permute-start.11 = (bf16[384,512]{1,0:T(8,128)(2,1)S(1)}, bf16[384,512]{1,0:T(8,128)(2,1)}, u32[]{:S(2)}, u32[]{:S(2)}) collective-permute-start(bf16[384,512]{1,0:T(8,128)(2,1)S(1)} %collective-permute-done.7.rest_4_), channel_id=1, source_target_pairs={{0,4},{4,0},{1,5},{5,1},{2,6},{6,2},{3,7},{7,3},{8,12},{12,8},{9,1... | collective-permute-start | bytes 1179656 | tf_op jit(solution)/shard_map/ppermute | solution.py:50
  84.2 4.7 %copy-start.4 = (bf16[384,512]{1,0:T(8,128)(2,1)}, bf16[384,512]{1,0:T(8,128)(2,1)S(1)}, u32[]{:S(2)}) copy-start(bf16[384,512]{1,0:T(8,128)(2,1)S(1)} %collective-permute-done.6.rest_3_) | copy-start | bytes 1179652
  84.2 9.6 %collective-permute-start.10 = (bf16[384,512]{1,0:T(8,128)(2,1)S(1)}, bf16[384,512]{1,0:T(8,128)(2,1)}, u32[]{:S(2)}, u32[]{:S(2)}) collective-permute-start(bf16[384,512]{1,0:T(8,128)(2,1)S(1)} %collective-permute-done.6.rest_3_), channel_id=1, source_target_pairs={{0,4},{4,0},{1,5},{5,1},{2,6},{6,2},{3,7},{7,3},{8,12},{12,8},{9,1... | collective-permute-start | bytes 1179656 | tf_op jit(solution)/shard_map/ppermute | solution.py:50
  88.8 5.0 %copy-start.1 = (s32[4]{0:T(128)S(1)}, s32[4]{0:T(128)}, u32[]{:S(2)}) copy-start(s32[4]{0:T(128)} %copy-done) | copy-start | bytes 52
  101.4 6.5 %collective-permute-start.12 = (bf16[128,384]{1,0:T(8,128)(2,1)S(1)}, bf16[128,384]{1,0:T(8,128)(2,1)S(1)}, u32[]{:S(2)}, u32[]{:S(2)}) collective-permute-start(bf16[128,384]{1,0:T(8,128)(2,1)S(1)} %get-tuple-element.65), channel_id=1, source_target_pairs={{0,1},{1,2},{2,3},{3,0},{4,5},{5,6},{6,7},{7,4},{8,9},{9,10},{10,1... | collective-permute-start | bytes 294920 | tf_op jit(solution)/shard_map/ppermute | solution.py:50
  101.5 7.8 %collective-permute-start.13 = (bf16[128,384]{1,0:T(8,128)(2,1)S(1)}, bf16[128,384]{1,0:T(8,128)(2,1)S(1)}, u32[]{:S(2)}, u32[]{:S(2)}) collective-permute-start(bf16[128,384]{1,0:T(8,128)(2,1)S(1)} %get-tuple-element.66), channel_id=1, source_target_pairs={{0,3},{1,0},{2,1},{3,2},{4,7},{5,4},{6,5},{7,6},{8,11},{9,8},{10,9... | collective-permute-start | bytes 294920 | tf_op jit(solution)/shard_map/ppermute | solution.py:50
  104.7 6.2 %collective-permute-start.14 = (bf16[128,384]{1,0:T(8,128)(2,1)S(1)}, bf16[128,384]{1,0:T(8,128)(2,1)S(1)}, u32[]{:S(2)}, u32[]{:S(2)}) collective-permute-start(bf16[128,384]{1,0:T(8,128)(2,1)S(1)} %get-tuple-element.67), channel_id=1, source_target_pairs={{0,2},{1,3},{2,0},{3,1},{4,6},{5,7},{6,4},{7,5},{8,10},{9,11},{10,... | collective-permute-start | bytes 294920 | tf_op jit(solution)/shard_map/ppermute | solution.py:50
where the time goes:
time: 113 us
  waiting for transfers between devices  52 us (46%)
  Pallas kernels  28.5 us (25%)
  starting transfers between devices  26.7 us (24%)
  local copies, waits for them, and re-layouts  5.4 us (5%)
    ppermute x15, waiting for transfers between devices, shifted(): lax.ppermute(array, axis, [(i, (i + by) % count) for i in range(count)])  49.2 us
    ppermute x15, starting transfers between devices, shifted(): lax.ppermute(array, axis, [(i, (i + by) % count) for i in range(count)])  13.7 us
    all_to_all x1, starting transfers between devices, local(): asked = lax.all_to_all(request, KV, 0, 0, tiled=True)  8.33 us
    pallas_call x1, Pallas kernels, attend_far(): pl.pallas_call(body, grid_spec=pltpu.PrefetchScalarGridSpec(num_scalar_pr...  7.54 us
    pallas_call x1, Pallas kernels, attend_own(): pl.pallas_call(body, grid=(heads,), in_specs=[column, column, pl.BlockSpe...  4.95 us
    pallas_call x1, Pallas kernels, project_query(): pl.pallas_call(body, grid_spec=pltpu.PrefetchScalarGridSpec(num_scalar_pr...  4.64 us
    all_to_all x1, starting transfers between devices, local(): got = lax.all_to_all(send, KV, split_axis=0, concat_axis=0, tiled=True)  4.62 us
    pallas_call x1, Pallas kernels, project_near(): pl.pallas_call(body, in_specs=[SMEM, HBM, VMEM, VMEM, HBM, HBM], out_spec...  4.57 us
  transfers between devices with their start and end apart: 17, of which 9 were waited for; matrix products, arithmetic and copies ran while one was open for 3% of the time, Pallas kernels for 13%

commit v1 on v0

--- a/solution.py
+++ b/solution.py
@@ -15,7 +15,6 @@
 NEG = -1e30
 LOG2E = 1.4426950408889634
 SMALL = 24 * 1024 * 1024
-LARGE = 60 * 1024 * 1024
 HBM = pl.BlockSpec(memory_space=pltpu.HBM)
 VMEM = pl.BlockSpec(memory_space=pltpu.VMEM)
 SMEM = pl.BlockSpec(memory_space=pltpu.SMEM)
@@ -50,13 +49,14 @@
     return lax.ppermute(array, axis, [(i, (i + by) % count) for i in range(count)])
 
 
-def project_near(where, own, left, right, w_key, w_value):
+def project_near(where, core, own, left, right, w_key, w_value, w_out):
     rows, feat = own.shape
     width = w_key.shape[1]
     chunks = where.shape[0]
-
-    def body(where_ref, own_hbm, l_ref, r_ref, wk_hbm, wv_hbm, tot_ref, wk_last, wv_last, l_hbm, r_hbm, *rest):
-        own_ref, chunk_refs, sems = rest
+    part = w_out.shape[1] // 4
+
+    def body(where_ref, core_ref, own_hbm, l_ref, r_ref, wk_hbm, wv_hbm, w_hbm, *rest):
+        tot_ref, wk_last, wv_last, l_hbm, r_hbm, low_ref, high_ref, own_ref, chunk_refs, sems = rest
         copies = []
 
         def fetch(src, dst):
@@ -73,6 +73,9 @@
         span = pl.ds(pl.multiple_of(where_ref[chunks - 1] * feat, feat), feat)
         last = [fetch(wk_hbm.at[span, :], wk_last), fetch(wv_hbm.at[span, :], wv_last)]
         last += [fetch(l_ref, l_hbm), fetch(r_ref, r_hbm)]
+        for k, ref in enumerate((low_ref, high_ref)):
+            at = pl.multiple_of((2 * core_ref[0] + k) * part, part)
+            last.append(fetch(w_hbm.at[:, pl.ds(at, part)], ref))
         own_copy.wait()
         for copy in pieces:
             copy.wait()
@@ -85,24 +88,26 @@
     chunk = (feat, width)
     return pl.pallas_call(
         body,
-        in_specs=[SMEM, HBM, VMEM, VMEM, HBM, HBM],
-        out_specs=[VMEM, VMEM, VMEM, HBM, HBM],
+        in_specs=[SMEM, SMEM, HBM, VMEM, VMEM, HBM, HBM, HBM],
+        out_specs=[VMEM, VMEM, VMEM, HBM, HBM, VMEM, VMEM],
         out_shape=[
             in_vmem((rows, 2 * width), jnp.float32),
             in_vmem(chunk, jnp.bfloat16),
             in_vmem(chunk, jnp.bfloat16),
             in_hbm((rows, feat), jnp.bfloat16),
             in_hbm((rows, feat), jnp.bfloat16),
+            in_vmem((w_out.shape[0], part), jnp.bfloat16),
+            in_vmem((w_out.shape[0], part), jnp.bfloat16),
         ],
         scratch_shapes=[
             pltpu.VMEM((rows, feat), jnp.bfloat16),
             pltpu.VMEM((chunks - 1, 2, feat, width), jnp.bfloat16),
-            pltpu.SemaphoreType.DMA((2 * chunks + 3,)),
+            pltpu.SemaphoreType.DMA((2 * chunks + 5,)),
         ],
         compiler_params=params(),
         cost_estimate=cost(12 * rows * feat * width, 20 * feat * width),
         name="project_near",
-    )(where, *keep_in_hbm(own), left, right, *keep_in_hbm(w_key, w_value))
+    )(where, core, *keep_in_hbm(own), left, right, *keep_in_hbm(w_key, w_value, w_out))
 
 
 def project_last(asked, top, bottom, wk_last, wv_last, total):
@@ -189,8 +194,8 @@
             in_specs=[toks, toks, toks, halves, halves, chunk(0), chunk(1), chunk(2), chunk(3)],
             out_specs=pl.BlockSpec((rows, width), lambda i, s: (0, 0)),
         ),
-        out_shape=in_hbm((rows, width), jnp.bfloat16),
-        compiler_params=params(LARGE),
+        out_shape=in_vmem((rows, width), jnp.bfloat16),
+        compiler_params=params(),
         cost_estimate=cost(8 * rows * feat * width, 16 * feat * width),
         name="project_query",
     )(where, *keep_in_hbm(own, left, right, top, bottom, w_query, w_query, w_query, w_query))
@@ -296,10 +301,10 @@
         ],
         out_specs=[column, column, column],
         out_shape=[in_hbm((rows, width), jnp.float32)] * 3,
-        compiler_params=params(LARGE),
+        compiler_params=params(),
         cost_estimate=cost(8 * rows * rows * width, 16 * rows * width, rows * rows * heads),
         name="attend_own",
-    )(query, pair, pair, mask)
+    )(query, *keep_in_hbm(pair, pair, mask))
 
 
 def attend_far(where, query, got, mask, high, total, summed, carried):
@@ -385,27 +390,28 @@
         compiler_params=params(),
         cost_estimate=cost(8 * rows * count * width, 4 * count * width, rows * count * heads),
         name="attend_far",
-    )(where, *keep_in_hbm(query), got, got, *keep_in_hbm(mask, high, total, summed, *carried))
+    )(where, query, got, got, *keep_in_hbm(mask, high, total, summed, *carried))
 
 
 def mix(core, attended, w_own, mine, other):
     rows, width = attended[0].shape
-    span = mine[0].shape[1]
-    part = mine[2].shape[1]
-
-    def body(core_ref, own_ref, l_ref, r_ref, f_ref, w_ref, *rest):
-        out_hbm, out_ref, sems = rest[8:]
+    part = mine[0].shape[1]
+
+    def body(core_ref, *rest):
+        own_ref, far_refs, w_ref, pieces = rest[0], rest[1:4], rest[4], (rest[5:11], rest[11:17])
+        out_hbm, out_ref, sems = rest[17:]
         copies = []
-        for side, pieces in enumerate((rest[:4], rest[4:8])):
-            at = pl.multiple_of((core_ref[0] if side == 0 else 1 - core_ref[0]) * span, span)
-            total = f32dot(own_ref[...], w_ref[:, pl.ds(at, span)])
-            total = total + f32dot(l_ref[...], pieces[0][...]) + f32dot(r_ref[...], pieces[1][...])
+        for side in range(2):
+            base = (core_ref[0] if side == 0 else 1 - core_ref[0]) * 2
             for k in range(2):
-                to = slice(k * part, (k + 1) * part)
-                value = total[:, to] + f32dot(f_ref[...], pieces[2 + k][...])
-                out_ref[side, :, to] = value.astype(jnp.bfloat16)
-            copies.append(pltpu.make_async_copy(out_ref.at[side], out_hbm.at[:, pl.ds(at, span)], sems.at[side]))
-            copies[-1].start()
+                span = pl.ds(pl.multiple_of((base + k) * part, part), part)
+                total = f32dot(own_ref[...], w_ref[:, span])
+                for g in range(3):
+                    total = total + f32dot(far_refs[g][...], pieces[side][2 * g + k][...])
+                at = 2 * side + k
+                out_ref[at] = total.astype(jnp.bfloat16)
+                copies.append(pltpu.make_async_copy(out_ref.at[at], out_hbm.at[:, span], sems.at[at]))
+                copies[-1].start()
         for copy in copies:
             copy.wait()
 
@@ -414,10 +420,10 @@
         body,
         in_specs=[SMEM] + [VMEM] * len(args),
         out_specs=HBM,
-        out_shape=in_hbm((rows, 2 * span), jnp.bfloat16),
-        scratch_shapes=[pltpu.VMEM((2, rows, span), jnp.bfloat16), pltpu.SemaphoreType.DMA((2,))],
-        compiler_params=params(),
-        cost_estimate=cost(16 * rows * width * span, 16 * width * span),
+        out_shape=in_hbm((rows, 4 * part), jnp.bfloat16),
+        scratch_shapes=[pltpu.VMEM((4, rows, part), jnp.bfloat16), pltpu.SemaphoreType.DMA((4,))],
+        compiler_params=params(),
+        cost_estimate=cost(32 * rows * width * part, 32 * width * part),
         name="mix",
     )(core, *args)
 
@@ -442,19 +448,20 @@
 
     top = shifted(left[:half], "tp", 1)
     bottom = shifted(right[half:], "tp", -1)
-    total, wk_last, wv_last, left, right = project_near(where, tokens, left, right, w_key, w_value)
+    total, wk_last, wv_last, left, right, low, high_part = project_near(
+        where, core, tokens, left, right, w_key, w_value, w_out
+    )
     pair, send, top, bottom = project_last(asked, top, bottom, wk_last, wv_last, total)
-    w_mine, send = lax.optimization_barrier((w_out, send))
+    low, high_part, send = lax.optimization_barrier((low, high_part, send))
     got = lax.all_to_all(send, KV, split_axis=0, concat_axis=0, tiled=True)
 
-    span = w_out.shape[1] // 2
-    part = span // 2
-    piece = lax.dynamic_slice_in_dim(w_mine, core[0] * span, span, axis=1)
-    w_left = shifted(piece, "tp", 1)
-    w_right = shifted(piece, "tp", -1)
-    w_low = shifted(w_left[:, :part], "tp", 1)
-    w_high = shifted(w_right[:, part:], "tp", -1)
-    mine = (w_left, w_right, w_low, w_high)
+    left_low = shifted(low, "tp", 1)
+    right_high = shifted(high_part, "tp", -1)
+    left_high = shifted(high_part, "tp", 1)
+    right_low = shifted(low, "tp", -1)
+    far_low = shifted(left_low, "tp", 1)
+    far_high = shifted(right_high, "tp", -1)
+    mine = (left_low, left_high, right_low, right_high, far_low, far_high)
     other = tuple(shifted(w, "kv_2", 1) for w in mine)
 
     query = project_query(where, tokens, left, right, top, bottom, w_query)
@@ -462,7 +469,7 @@
     weights = (w_out, *mine, *other)
     outs = attend_far(where, query, got.reshape(-1, 2 * width), mask, high, totals, summed, weights)
     attended = (outs[0], shifted(outs[2], "tp", 1), shifted(outs[1], "tp", -1), shifted(outs[3], "tp", 2))
-    return mix(core, attended, outs[4], outs[5:9], outs[9:])
+    return mix(core, attended, outs[4], outs[5:11], outs[11:])
 
 
 def solution(mesh):

time: 113 us -> 109 us (0.965)
  waiting for transfers between devices: 52 us -> 42.8 us
  starting transfers between devices: 26.7 us -> 32.3 us
    ppermute x15 -> x19, waiting for transfers between devices: 49.2 us -> 41.2 us  [shifted(): lax.ppermute(array, axis, [(i, (i + by) % count) for i in range(count)])]
    ppermute x15 -> x19, starting transfers between devices: 13.7 us -> 17.6 us  [shifted(): lax.ppermute(array, axis, [(i, (i + by) % count) for i in range(count)])]
    unnamed x10 -> x30, local copies, waits for them, and re-layouts: 0.71 us -> 3.97 us
    slice x2 -> x0, local copies, waits for them, and re-layouts: 2.04 us -> none  [the longest x1 1.02 us: local(): w_low = shifted(w_left[:, :part], 'tp', 1)]
    all_to_all x1, starting transfers between devices: 4.62 us -> 6.31 us  [local(): got = lax.all_to_all(send, KV, split_axis=0, concat_axis=0, tiled=True)]
    all_to_all x1, waiting for transfers between devices: 2.79 us -> 1.22 us  [local(): asked = lax.all_to_all(request, KV, 0, 0, tiled=True)]
    dynamic_slice x1 -> x0, local copies, waits for them, and re-layouts: 1.19 us -> none  [local(): piece = lax.dynamic_slice_in_dim(w_mine, core[0] * span, span, axis=1)]
  transfers between devices with their start and end apart: 17 -> 21, of which waited for: 9 -> 12; matrix products, arithmetic and copies ran while one was open for 3% -> 0% of each run, Pallas kernels for 13% -> 13%
where the time goes in v1:
time: 109 us; the launch traced here: 108 us
  waiting for transfers between devices  42.8 us (39%)
  starting transfers between devices  32.3 us (30%)
  Pallas kernels  27.4 us (25%)
  local copies, waits for them, and re-layouts  5.41 us (5%)
    ppermute x19, waiting for transfers between devices, shifted(): lax.ppermute(array, axis, [(i, (i + by) % count) for i in range(count)])  41.2 us
    ppermute x19, starting transfers between devices, shifted(): lax.ppermute(array, axis, [(i, (i + by) % count) for i in range(count)])  17.6 us
    all_to_all x1, starting transfers between devices, local(): asked = lax.all_to_all(request, KV, 0, 0, tiled=True)  8.33 us
    pallas_call x1, Pallas kernels, attend_far(): pl.pallas_call(body, grid_spec=pltpu.PrefetchScalarGridSpec(num_scalar_pr...  7.59 us
    all_to_all x1, starting transfers between devices, local(): got = lax.all_to_all(send, KV, split_axis=0, concat_axis=0, tiled=True)  6.31 us
    pallas_call x1, Pallas kernels, attend_own(): pl.pallas_call(body, grid=(heads,), in_specs=[column, column, pl.BlockSpe...  4.71 us
    pallas_call x1, Pallas kernels, project_near(): pl.pallas_call(body, in_specs=[SMEM, SMEM, HBM, VMEM, VMEM, HBM, HBM, HBM...  4.59 us
    unnamed x30, local copies, waits for them, and re-layouts  3.97 us
  transfers between devices with their start and end apart: 21, of which 12 were waited for; matrix products, arithmetic and copies ran while one was open for 0% of the time, Pallas kernels for 13%

profile of v1, /device:TPU:0, one launch (start us, length us, event | category | flops | bytes accessed | tf_op | source)
XLA Modules:
  0.0 108.3 jit_solution(4135423993164150981)
XLA Ops:
  0.1 2.9 %collective-permute-start.1 = (bf16[512,512]{1,0:T(8,128)(2,1)}, bf16[512,512]{1,0:T(8,128)(2,1)S(1)}, u32[]{:S(2)}, u32[]{:S(2)}) collective-permute-start(bf16[512,512]{1,0:T(8,128)(2,1)} %o_ref), channel_id=1, source_target_pairs={{0,3},{1,0},{2,1},{3,2},{4,7},{5,4},{6,5},{7,6},{8,11},{9,8},{10,9... | collective-permute-start | bytes 1572872 | tf_op jit(solution)/shard_map/ppermute | solution.py:49
  3.0 0.7 copy-done
  3.7 1.0 plan.1
  4.6 9.8 %collective-permute-done.1.r_ref = bf16[512,512]{1,0:T(8,128)(2,1)S(1)} collective-permute-done((bf16[512,512]{1,0:T(8,128)(2,1)}, bf16[512,512]{1,0:T(8,128)(2,1)S(1)}, u32[]{:S(2)}, u32[]{:S(2)}) %collective-permute-start.1) | collective-permute-done | bytes 524320 | tf_op jit(solution)/shard_map/ppermute | solution.py:49
  14.5 3.3 %collective-permute-done.l_ref = bf16[512,512]{1,0:T(8,128)(2,1)S(1)} collective-permute-done((bf16[512,512]{1,0:T(8,128)(2,1)}, bf16[512,512]{1,0:T(8,128)(2,1)S(1)}, u32[]{:S(2)}, u32[]{:S(2)}) %collective-permute-start) | collective-permute-done | bytes 524320 | tf_op jit(solution)/shard_map/ppermute | solution.py:49
  17.8 0.7 slice.6
  18.5 0.7 slice.7
  19.5 1.7 %collective-permute-start.2 = (bf16[256,512]{1,0:T(8,128)(2,1)}, bf16[256,512]{1,0:T(8,128)(2,1)}, u32[]{:S(2)}, u32[]{:S(2)}) collective-permute-start(bf16[256,512]{1,0:T(8,128)(2,1)} %slice.6), channel_id=1, source_target_pairs={{0,1},{1,2},{2,3},{3,0},{4,5},{5,6},{6,7},{7,4},{8,9},{9,10},{10,1... | collective-permute-start | bytes 786440 | tf_op jit(solution)/shard_map/ppermute | solution.py:49
  21.2 8.3 %all-to-all-start = ((s32[32,1,128]{2,1,0:T(1,128)}), s32[32,1,128]{2,1,0:T(1,128)S(1)}, u32[]{:S(2)}, u32[]{:S(2)}) async-start(s32[32,1,128]{2,1,0:T(1,128)} %bitcast.14), calls=%async_computation | async-start | bytes 32768 | tf_op jit(solution)/shard_map/all_to_all | solution.py:446
  29.6 4.6 %project_near.1 = (f32[512,768]{1,0:T(8,128)S(1)}, bf16[512,384]{1,0:T(8,128)(2,1)S(1)}, bf16[512,384]{1,0:T(8,128)(2,1)S(1)}, bf16[512,512]{1,0:T(8,128)(2,1)},...) custom-call(s32[4]{0:T(128)S(1)} %pad_add_fusion.where_ref, ...), custom_call_target="tpu_custom_call" | custom-call | flops 1207959552 | bytes 3932160 | tf_op jit(solution)/shard_map/project_near/pallas_call | solution.py:89
  34.2 0.8 copy-done.1
  35.0 0.8 copy-done.3
  35.7 1.2 %all-to-all-done = s32[32,1,128]{2,1,0:T(1,128)S(1)} async-done(((s32[32,1,128]{2,1,0:T(1,128)}), s32[32,1,128]{2,1,0:T(1,128)S(1)}, u32[]{:S(2)}, u32[]{:S(2)}) %all-to-all-start) | async-done | bytes 16416 | tf_op jit(solution)/shard_map/all_to_all | solution.py:446
  37.0 3.8 %project_last.1 = (bf16[512,768]{1,0:T(8,128)(2,1)}, bf16[64,32,768]{2,1,0:T(8,128)(2,1)}, bf16[256,512]{1,0:T(8,128)(2,1)}, bf16[256,512]{1,0:T(8,128)(2,1)}) custom-call(s32[32,128]{1,0:T(8,128)S(1)} %bitcast.13, bf16[256,512]{1,0:T(8,128)(2,1)} %collective-permute-done.2.t_ref, bf16[256,512]{1,0:T(8,128)(2,1)} %collective-permute-done.3.b_ref, ...), custom_call_target="tpu_custom_call" | custom-call | flops 402653184 | bytes 2359296 | tf_op jit(solution)/shard_map/project_last/pallas_call | solution.py:149
  40.8 6.3 %all-to-all-start.1 = ((bf16[64,32,768]{2,1,0:T(8,128)(2,1)}), bf16[64,32,768]{2,1,0:T(8,128)(2,1)S(1)}, u32[]{:S(2)}, u32[]{:S(2)}) async-start(bf16[64,32,768]{2,1,0:T(8,128)(2,1)} %get-tuple-element.66), calls=%async_computation.1 | async-start | bytes 6291456 | tf_op jit(solution)/shard_map/all_to_all | solution.py:456
  47.1 1.6 %collective-permute-start.6 = (bf16[384,512]{1,0:T(8,128)(2,1)}, bf16[384,512]{1,0:T(8,128)(2,1)S(1)}, u32[]{:S(2)}, u32[]{:S(2)}) collective-permute-start(bf16[384,512]{1,0:T(8,128)(2,1)} %copy-done.3), channel_id=1, source_target_pairs={{0,3},{1,0},{2,1},{3,2},{4,7},{5,4},{6,5},{7,6},{8,11},{9,8},{10,9... | collective-permute-start | bytes 1179656 | tf_op jit(solution)/shard_map/ppermute | solution.py:49
  49.2 2.7 %collective-permute-start.7 = (bf16[384,512]{1,0:T(8,128)(2,1)S(1)}, bf16[384,512]{1,0:T(8,128)(2,1)S(1)}, u32[]{:S(2)}, u32[]{:S(2)}) collective-permute-start(bf16[384,512]{1,0:T(8,128)(2,1)S(1)} %copy-done.2), channel_id=1, source_target_pairs={{0,3},{1,0},{2,1},{3,2},{4,7},{5,4},{6,5},{7,6},{8,11},{9,8},{10,9... | collective-permute-start | bytes 1179656 | tf_op jit(solution)/shard_map/ppermute | solution.py:49
  51.9 7.5 %collective-permute-done.6.rest_3_ = bf16[384,512]{1,0:T(8,128)(2,1)S(1)} collective-permute-done((bf16[384,512]{1,0:T(8,128)(2,1)}, bf16[384,512]{1,0:T(8,128)(2,1)S(1)}, u32[]{:S(2)}, u32[]{:S(2)}) %collective-permute-start.6) | collective-permute-done | bytes 393248 | tf_op jit(solution)/shard_map/ppermute | solution.py:49
  59.4 2.7 %collective-permute-done.4.rest_1_ = bf16[384,512]{1,0:T(8,128)(2,1)S(1)} collective-permute-done((bf16[384,512]{1,0:T(8,128)(2,1)}, bf16[384,512]{1,0:T(8,128)(2,1)S(1)}, u32[]{:S(2)}, u32[]{:S(2)}) %collective-permute-start.4) | collective-permute-done | bytes 393248 | tf_op jit(solution)/shard_map/ppermute | solution.py:49
  62.1 5.0 %collective-permute-done.7.rest_4_ = bf16[384,512]{1,0:T(8,128)(2,1)S(1)} collective-permute-done((bf16[384,512]{1,0:T(8,128)(2,1)S(1)}, bf16[384,512]{1,0:T(8,128)(2,1)S(1)}, u32[]{:S(2)}, u32[]{:S(2)}) %collective-permute-start.7) | collective-permute-done | bytes 393248 | tf_op jit(solution)/shard_map/ppermute | solution.py:49
  67.1 2.7 %collective-permute-start.9 = (bf16[384,512]{1,0:T(8,128)(2,1)S(1)}, bf16[384,512]{1,0:T(8,128)(2,1)S(1)}, u32[]{:S(2)}, u32[]{:S(2)}) collective-permute-start(bf16[384,512]{1,0:T(8,128)(2,1)S(1)} %collective-permute-done.7.rest_4_), channel_id=1, source_target_pairs={{0,3},{1,0},{2,1},{3,2},{4,7},{5,4},{6,5},{7,6},{8,11},{9,8},{10,9... | collective-permute-start | bytes 1179656 | tf_op jit(solution)/shard_map/ppermute | solution.py:49
  71.1 6.9 %collective-permute-done.8.rest_5_ = bf16[384,512]{1,0:T(8,128)(2,1)S(1)} collective-permute-done((bf16[384,512]{1,0:T(8,128)(2,1)S(1)}, bf16[384,512]{1,0:T(8,128)(2,1)S(1)}, u32[]{:S(2)}, u32[]{:S(2)}) %collective-permute-start.8) | collective-permute-done | bytes 393248 | tf_op jit(solution)/shard_map/ppermute | solution.py:49
  78.5 3.8 %project_query.1.q_ref = bf16[512,384]{1,0:T(8,128)(2,1)S(1)} custom-call(s32[4]{0:T(128)S(1)} %pad_add_fusion.where_ref, bf16[512,512]{1,0:T(8,128)(2,1)} %o_ref, bf16[512,512]{1,0:T(8,128)(2,1)} %get-tuple-element.56.l_ref, bf16[512,512]{1,0:T(8,128)(2,1)} %get-tuple-element.57.r_ref, bf16[256,512]{1,0:T(8,128)(2,1)} %get-tuple-element.61.t_ref, ...), custom_call_target="tpu_custom_call" | custom-call | flops 805306368 | bytes 3145728 | tf_op jit(solution)/shard_map/project_query/pallas_call | solution.py:189
  82.3 4.7 %attend_own.1 = (f32[512,384]{1,0:T(8,128)}, f32[512,384]{1,0:T(8,128)}, f32[512,384]{1,0:T(8,128)}) custom-call(bf16[512,384]{1,0:T(8,128)(2,1)S(1)} %project_query.1.q_ref, bf16[512,768]{1,0:T(8,128)(2,1)} %get-tuple-element.68.k_ref.v_ref, bf16[512,768]{1,0:T(8,128)(2,1)} %get-tuple-element.68.k_ref.v_ref, bf16[512,128]{1,0:T(8,128)(2,1)} %get-tuple-element.67.mask_ref), custom_call_target="tpu_custom_call" | custom-call | flops 805306368 | bytes 3145728 | tf_op jit(solution)/shard_map/attend_own/pallas_call | solution.py:293
  88.1 0.7 copy-done.14
  89.1 7.6 %attend_far.1 = (bf16[128,384]{1,0:T(8,128)(2,1)S(1)}, bf16[128,384]{1,0:T(8,128)(2,1)S(1)}, bf16[128,384]{1,0:T(8,128)(2,1)S(1)}, bf16[128,384]{1,0:T(8,128)(2,...) custom-call(s32[4]{0:T(128)S(1)} %pad_add_fusion.where_ref, ...), custom_call_target="tpu_custom_call" | custom-call | flops 3221225472 | bytes 3145728 | tf_op jit(solution)/shard_map/attend_far/pallas_call | solution.py:369
  96.8 3.2 %collective-permute-start.17 = (bf16[128,384]{1,0:T(8,128)(2,1)S(1)}, bf16[128,384]{1,0:T(8,128)(2,1)S(1)}, u32[]{:S(2)}, u32[]{:S(2)}) collective-permute-start(bf16[128,384]{1,0:T(8,128)(2,1)S(1)} %get-tuple-element.76), channel_id=1, source_target_pairs={{0,3},{1,0},{2,1},{3,2},{4,7},{5,4},{6,5},{7,6},{8,11},{9,8},{10,9... | collective-permute-start | bytes 294920 | tf_op jit(solution)/shard_map/ppermute | solution.py:49
  100.0 0.9 collective-permute-start.18
  101.0 2.0 %collective-permute-done.16.rest_1_ = bf16[128,384]{1,0:T(8,128)(2,1)S(1)} collective-permute-done((bf16[128,384]{1,0:T(8,128)(2,1)S(1)}, bf16[128,384]{1,0:T(8,128)(2,1)S(1)}, u32[]{:S(2)}, u32[]{:S(2)}) %collective-permute-start.16) | collective-permute-done | bytes 98336 | tf_op jit(solution)/shard_map/ppermute | solution.py:49
  103.0 1.5 %collective-permute-done.17.rest_2_ = bf16[128,384]{1,0:T(8,128)(2,1)S(1)} collective-permute-done((bf16[128,384]{1,0:T(8,128)(2,1)S(1)}, bf16[128,384]{1,0:T(8,128)(2,1)S(1)}, u32[]{:S(2)}, u32[]{:S(2)}) %collective-permute-start.17) | collective-permute-done | bytes 98336 | tf_op jit(solution)/shard_map/ppermute | solution.py:49
  104.4 1.8 %collective-permute-done.18.rest_3_ = bf16[128,384]{1,0:T(8,128)(2,1)S(1)} collective-permute-done((bf16[128,384]{1,0:T(8,128)(2,1)S(1)}, bf16[128,384]{1,0:T(8,128)(2,1)S(1)}, u32[]{:S(2)}, u32[]{:S(2)}) %collective-permute-start.18) | collective-permute-done | bytes 98336 | tf_op jit(solution)/shard_map/ppermute | solution.py:49
  106.2 1.9 %mix.1 = bf16[128,2048]{1,0:T(8,128)(2,1)} custom-call(s32[1]{0:T(128)} %bitcast.5.core_ref, bf16[128,384]{1,0:T(8,128)(2,1)S(1)} %get-tuple-element.74.rest_0_, bf16[128,384]{1,0:T(8,128)(2,1)S(1)} %collective-permute-done.16.rest_1_, bf16[128,384]{1,0:T(8,128)(2,1)S(1)} %collective-permute-done.17.rest_2_, ...), custom_call_target="tpu_custom_call" | custom-call | flops 805306368 | bytes 6291456 | tf_op jit(solution)/shard_map/mix/pallas_call | solution.py:419
  (50 shorter events, 4.0 us)
Async XLA Ops:
  0.1 14.4 %collective-permute-start.1 = (bf16[512,512]{1,0:T(8,128)(2,1)}, bf16[512,512]{1,0:T(8,128)(2,1)S(1)}, u32[]{:S(2)}, u32[]{:S(2)}) collective-permute-start(bf16[512,512]{1,0:T(8,128)(2,1)} %o_ref), channel_id=1, source_target_pairs={{0,3},{1,0},{2,1},{3,2},{4,7},{5,4},{6,5},{7,6},{8,11},{9,8},{10,9... | collective-permute-start | bytes 1572872 | tf_op jit(solution)/shard_map/ppermute | solution.py:49
  3.0 14.8 %collective-permute-start = (bf16[512,512]{1,0:T(8,128)(2,1)}, bf16[512,512]{1,0:T(8,128)(2,1)S(1)}, u32[]{:S(2)}, u32[]{:S(2)}) collective-permute-start(bf16[512,512]{1,0:T(8,128)(2,1)} %o_ref), channel_id=1, source_target_pairs={{0,1},{1,2},{2,3},{3,0},{4,5},{5,6},{6,7},{7,4},{8,9},{9,10},{10,1... | collective-permute-start | bytes 1572872 | tf_op jit(solution)/shard_map/ppermute | solution.py:49
  19.2 17.7 %collective-permute-start.3 = (bf16[256,512]{1,0:T(8,128)(2,1)}, bf16[256,512]{1,0:T(8,128)(2,1)}, u32[]{:S(2)}, u32[]{:S(2)}) collective-permute-start(bf16[256,512]{1,0:T(8,128)(2,1)} %slice.7), channel_id=1, source_target_pairs={{0,3},{1,0},{2,1},{3,2},{4,7},{5,4},{6,5},{7,6},{8,11},{9,8},{10,9... | collective-permute-start | bytes 786440 | tf_op jit(solution)/shard_map/ppermute | solution.py:49
  19.5 17.5 %collective-permute-start.2 = (bf16[256,512]{1,0:T(8,128)(2,1)}, bf16[256,512]{1,0:T(8,128)(2,1)}, u32[]{:S(2)}, u32[]{:S(2)}) collective-permute-start(bf16[256,512]{1,0:T(8,128)(2,1)} %slice.6), channel_id=1, source_target_pairs={{0,1},{1,2},{2,3},{3,0},{4,5},{5,6},{6,7},{7,4},{8,9},{9,10},{10,1... | collective-permute-start | bytes 786440 | tf_op jit(solution)/shard_map/ppermute | solution.py:49
  21.2 15.7 %all-to-all-start = ((s32[32,1,128]{2,1,0:T(1,128)}), s32[32,1,128]{2,1,0:T(1,128)S(1)}, u32[]{:S(2)}, u32[]{:S(2)}) async-start(s32[32,1,128]{2,1,0:T(1,128)} %bitcast.14), calls=%async_computation | async-start | bytes 32768 | tf_op jit(solution)/shard_map/all_to_all | solution.py:446
  34.2 0.8 copy-start.1
  40.8 8.4 %copy-start.2 = (bf16[384,512]{1,0:T(8,128)(2,1)S(1)}, bf16[384,512]{1,0:T(8,128)(2,1)}, u32[]{:S(2)}) copy-start(bf16[384,512]{1,0:T(8,128)(2,1)} %copy-done.1) | copy-start | bytes 1179652
  40.8 48.3 %all-to-all-start.1 = ((bf16[64,32,768]{2,1,0:T(8,128)(2,1)}), bf16[64,32,768]{2,1,0:T(8,128)(2,1)S(1)}, u32[]{:S(2)}, u32[]{:S(2)}) async-start(bf16[64,32,768]{2,1,0:T(8,128)(2,1)} %get-tuple-element.66), calls=%async_computation.1 | async-start | bytes 6291456 | tf_op jit(solution)/shard_map/all_to_all | solution.py:456
  47.1 12.3 %collective-permute-start.6 = (bf16[384,512]{1,0:T(8,128)(2,1)}, bf16[384,512]{1,0:T(8,128)(2,1)S(1)}, u32[]{:S(2)}, u32[]{:S(2)}) collective-permute-start(bf16[384,512]{1,0:T(8,128)(2,1)} %copy-done.3), channel_id=1, source_target_pairs={{0,3},{1,0},{2,1},{3,2},{4,7},{5,4},{6,5},{7,6},{8,11},{9,8},{10,9... | collective-permute-start | bytes 1179656 | tf_op jit(solution)/shard_map/ppermute | solution.py:49
  48.7 13.4 %collective-permute-start.4 = (bf16[384,512]{1,0:T(8,128)(2,1)}, bf16[384,512]{1,0:T(8,128)(2,1)S(1)}, u32[]{:S(2)}, u32[]{:S(2)}) collective-permute-start(bf16[384,512]{1,0:T(8,128)(2,1)} %copy-done.3), channel_id=1, source_target_pairs={{0,1},{1,2},{2,3},{3,0},{4,5},{5,6},{6,7},{7,4},{8,9},{9,10},{10,1... | collective-permute-start | bytes 1179656 | tf_op jit(solution)/shard_map/ppermute | solution.py:49
  49.2 17.9 %collective-permute-start.7 = (bf16[384,512]{1,0:T(8,128)(2,1)S(1)}, bf16[384,512]{1,0:T(8,128)(2,1)S(1)}, u32[]{:S(2)}, u32[]{:S(2)}) collective-permute-start(bf16[384,512]{1,0:T(8,128)(2,1)S(1)} %copy-done.2), channel_id=1, source_target_pairs={{0,3},{1,0},{2,1},{3,2},{4,7},{5,4},{6,5},{7,6},{8,11},{9,8},{10,9... | collective-permute-start | bytes 1179656 | tf_op jit(solution)/shard_map/ppermute | solution.py:49
  51.9 18.6 %collective-permute-start.5 = (bf16[384,512]{1,0:T(8,128)(2,1)S(1)}, bf16[384,512]{1,0:T(8,128)(2,1)S(1)}, u32[]{:S(2)}, u32[]{:S(2)}) collective-permute-start(bf16[384,512]{1,0:T(8,128)(2,1)S(1)} %copy-done.2), channel_id=1, source_target_pairs={{0,1},{1,2},{2,3},{3,0},{4,5},{5,6},{6,7},{7,4},{8,9},{9,10},{10,1... | collective-permute-start | bytes 1179656 | tf_op jit(solution)/shard_map/ppermute | solution.py:49
  59.4 19.1 %copy-start.4 = (bf16[384,512]{1,0:T(8,128)(2,1)}, bf16[384,512]{1,0:T(8,128)(2,1)S(1)}, u32[]{:S(2)}) copy-start(bf16[384,512]{1,0:T(8,128)(2,1)S(1)} %collective-permute-done.6.rest_3_) | copy-start | bytes 1179652
  59.4 11.1 %collective-permute-start.12 = (bf16[384,512]{1,0:T(8,128)(2,1)S(1)}, bf16[384,512]{1,0:T(8,128)(2,1)S(1)}, u32[]{:S(2)}, u32[]{:S(2)}) collective-permute-start(bf16[384,512]{1,0:T(8,128)(2,1)S(1)} %collective-permute-done.6.rest_3_), channel_id=1, source_target_pairs={{0,4},{4,0},{1,5},{5,1},{2,6},{6,2},{3,7},{7,3},{8,12},{12,8},{9,1... | collective-permute-start | bytes 1179656 | tf_op jit(solution)/shard_map/ppermute | solution.py:49
  62.1 20.2 %copy-start.5 = (bf16[384,512]{1,0:T(8,128)(2,1)}, bf16[384,512]{1,0:T(8,128)(2,1)S(1)}, u32[]{:S(2)}) copy-start(bf16[384,512]{1,0:T(8,128)(2,1)S(1)} %collective-permute-done.4.rest_1_) | copy-start | bytes 1179652
  62.1 15.9 %collective-permute-start.8 = (bf16[384,512]{1,0:T(8,128)(2,1)S(1)}, bf16[384,512]{1,0:T(8,128)(2,1)S(1)}, u32[]{:S(2)}, u32[]{:S(2)}) collective-permute-start(bf16[384,512]{1,0:T(8,128)(2,1)S(1)} %collective-permute-done.4.rest_1_), channel_id=1, source_target_pairs={{0,1},{1,2},{2,3},{3,0},{4,5},{5,6},{6,7},{7,4},{8,9},{9,10},{10,1... | collective-permute-start | bytes 1179656 | tf_op jit(solution)/shard_map/ppermute | solution.py:49
  67.1 15.2 %copy-start.6 = (bf16[384,512]{1,0:T(8,128)(2,1)}, bf16[384,512]{1,0:T(8,128)(2,1)S(1)}, u32[]{:S(2)}) copy-start(bf16[384,512]{1,0:T(8,128)(2,1)S(1)} %collective-permute-done.7.rest_4_) | copy-start | bytes 1179652
  67.1 10.9 %collective-permute-start.9 = (bf16[384,512]{1,0:T(8,128)(2,1)S(1)}, bf16[384,512]{1,0:T(8,128)(2,1)S(1)}, u32[]{:S(2)}, u32[]{:S(2)}) collective-permute-start(bf16[384,512]{1,0:T(8,128)(2,1)S(1)} %collective-permute-done.7.rest_4_), channel_id=1, source_target_pairs={{0,3},{1,0},{2,1},{3,2},{4,7},{5,4},{6,5},{7,6},{8,11},{9,8},{10,9... | collective-permute-start | bytes 1179656 | tf_op jit(solution)/shard_map/ppermute | solution.py:49
  69.8 17.2 %collective-permute-start.10 = (bf16[384,512]{1,0:T(8,128)(2,1)S(1)}, bf16[384,512]{1,0:T(8,128)(2,1)S(1)}, u32[]{:S(2)}, u32[]{:S(2)}) collective-permute-start(bf16[384,512]{1,0:T(8,128)(2,1)S(1)} %collective-permute-done.4.rest_1_), channel_id=1, source_target_pairs={{0,4},{4,0},{1,5},{5,1},{2,6},{6,2},{3,7},{7,3},{8,12},{12,8},{9,1... | collective-permute-start | bytes 1179656 | tf_op jit(solution)/shard_map/ppermute | solution.py:49
  70.5 11.8 %copy-start.7 = (bf16[384,512]{1,0:T(8,128)(2,1)}, bf16[384,512]{1,0:T(8,128)(2,1)S(1)}, u32[]{:S(2)}) copy-start(bf16[384,512]{1,0:T(8,128)(2,1)S(1)} %collective-permute-done.5.rest_2_) | copy-start | bytes 1179652
  70.5 16.5 %collective-permute-start.13 = (bf16[384,512]{1,0:T(8,128)(2,1)S(1)}, bf16[384,512]{1,0:T(8,128)(2,1)S(1)}, u32[]{:S(2)}, u32[]{:S(2)}) collective-permute-start(bf16[384,512]{1,0:T(8,128)(2,1)S(1)} %collective-permute-done.7.rest_4_), channel_id=1, source_target_pairs={{0,4},{4,0},{1,5},{5,1},{2,6},{6,2},{3,7},{7,3},{8,12},{12,8},{9,1... | collective-permute-start | bytes 1179656 | tf_op jit(solution)/shard_map/ppermute | solution.py:49
  70.5 8.0 %copy-start.8 = (bf16[384,512]{1,0:T(8,128)(2,1)}, bf16[384,512]{1,0:T(8,128)(2,1)S(1)}, u32[]{:S(2)}) copy-start(bf16[384,512]{1,0:T(8,128)(2,1)S(1)} %collective-permute-done.12.rest_9_) | copy-start | bytes 1179652
  70.6 16.5 %collective-permute-start.11 = (bf16[384,512]{1,0:T(8,128)(2,1)S(1)}, bf16[384,512]{1,0:T(8,128)(2,1)S(1)}, u32[]{:S(2)}, u32[]{:S(2)}) collective-permute-start(bf16[384,512]{1,0:T(8,128)(2,1)S(1)} %collective-permute-done.5.rest_2_), channel_id=1, source_target_pairs={{0,4},{4,0},{1,5},{5,1},{2,6},{6,2},{3,7},{7,3},{8,12},{12,8},{9,1... | collective-permute-start | bytes 1179656 | tf_op jit(solution)/shard_map/ppermute | solution.py:49
  78.0 4.3 %copy-start.9 = (bf16[384,512]{1,0:T(8,128)(2,1)}, bf16[384,512]{1,0:T(8,128)(2,1)S(1)}, u32[]{:S(2)}) copy-start(bf16[384,512]{1,0:T(8,128)(2,1)S(1)} %collective-permute-done.8.rest_5_) | copy-start | bytes 1179652
  78.0 9.1 %collective-permute-start.14 = (bf16[384,512]{1,0:T(8,128)(2,1)S(1)}, bf16[384,512]{1,0:T(8,128)(2,1)S(1)}, u32[]{:S(2)}, u32[]{:S(2)}) collective-permute-start(bf16[384,512]{1,0:T(8,128)(2,1)S(1)} %collective-permute-done.8.rest_5_), channel_id=1, source_target_pairs={{0,4},{4,0},{1,5},{5,1},{2,6},{6,2},{3,7},{7,3},{8,12},{12,8},{9,1... | collective-permute-start | bytes 1179656 | tf_op jit(solution)/shard_map/ppermute | solution.py:49
  78.0 4.3 %copy-start.10 = (bf16[384,512]{1,0:T(8,128)(2,1)}, bf16[384,512]{1,0:T(8,128)(2,1)S(1)}, u32[]{:S(2)}) copy-start(bf16[384,512]{1,0:T(8,128)(2,1)S(1)} %collective-permute-done.9.rest_6_) | copy-start | bytes 1179652
  78.0 10.8 %collective-permute-start.15 = (bf16[384,512]{1,0:T(8,128)(2,1)S(1)}, bf16[384,512]{1,0:T(8,128)(2,1)}, u32[]{:S(2)}, u32[]{:S(2)}) collective-permute-start(bf16[384,512]{1,0:T(8,128)(2,1)S(1)} %collective-permute-done.9.rest_6_), channel_id=1, source_target_pairs={{0,4},{4,0},{1,5},{5,1},{2,6},{6,2},{3,7},{7,3},{8,12},{12,8},{9,1... | collective-permute-start | bytes 1179656 | tf_op jit(solution)/shard_map/ppermute | solution.py:49
  87.1 0.8 copy-start.12
  87.1 1.0 copy-start.13
  96.7 6.2 %collective-permute-start.16 = (bf16[128,384]{1,0:T(8,128)(2,1)S(1)}, bf16[128,384]{1,0:T(8,128)(2,1)S(1)}, u32[]{:S(2)}, u32[]{:S(2)}) collective-permute-start(bf16[128,384]{1,0:T(8,128)(2,1)S(1)} %get-tuple-element.75), channel_id=1, source_target_pairs={{0,1},{1,2},{2,3},{3,0},{4,5},{5,6},{6,7},{7,4},{8,9},{9,10},{10,1... | collective-permute-start | bytes 294920 | tf_op jit(solution)/shard_map/ppermute | solution.py:49
  96.8 7.6 %collective-permute-start.17 = (bf16[128,384]{1,0:T(8,128)(2,1)S(1)}, bf16[128,384]{1,0:T(8,128)(2,1)S(1)}, u32[]{:S(2)}, u32[]{:S(2)}) collective-permute-start(bf16[128,384]{1,0:T(8,128)(2,1)S(1)} %get-tuple-element.76), channel_id=1, source_target_pairs={{0,3},{1,0},{2,1},{3,2},{4,7},{5,4},{6,5},{7,6},{8,11},{9,8},{10,9... | collective-permute-start | bytes 294920 | tf_op jit(solution)/shard_map/ppermute | solution.py:49
  100.0 6.2 %collective-permute-start.18 = (bf16[128,384]{1,0:T(8,128)(2,1)S(1)}, bf16[128,384]{1,0:T(8,128)(2,1)S(1)}, u32[]{:S(2)}, u32[]{:S(2)}) collective-permute-start(bf16[128,384]{1,0:T(8,128)(2,1)S(1)} %get-tuple-element.77), channel_id=1, source_target_pairs={{0,2},{1,3},{2,0},{3,1},{4,6},{5,7},{6,4},{7,5},{8,10},{9,11},{10,... | collective-permute-start | bytes 294920 | tf_op jit(solution)/shard_map/ppermute | solution.py:49
  (4 other events, 2.9 us)

commit v2 on v1

--- a/solution.py
+++ b/solution.py
@@ -13,7 +13,7 @@
 KV = ("kv_0", "kv_1", "kv_2")
 KV_TP = ("kv_0", "kv_1", "kv_2", "tp")
 NEG = -1e30
-LOG2E = 1.4426950408889634
+SCALE = HD ** (-0.5) * 1.4426950408889634
 SMALL = 24 * 1024 * 1024
 HBM = pl.BlockSpec(memory_space=pltpu.HBM)
 VMEM = pl.BlockSpec(memory_space=pltpu.VMEM)
@@ -268,10 +268,10 @@
 def attend_own(query, pair, mask, first_slot):
     rows, width = query.shape
     heads = width // HD
-    scale = HD ** (-0.5) * LOG2E
     tile = 256
 
-    def body(q_ref, k_ref, v_ref, mask_ref, high_ref, tot_ref, sum_ref):
+    def body(q_ref, k_ref, v_ref, mask_ref, sum_ref, log_ref):
+        head = pl.program_id(0)
         keys = jnp.concatenate([k_ref[...], one_hot(rows, first_slot)], axis=1)
         values = jnp.concatenate([v_ref[...], jnp.ones_like(v_ref)], axis=1)
         for lo in range(0, rows, tile):
@@ -282,150 +282,195 @@
             row = lax.broadcasted_iota(jnp.int32, scores.shape, 0) + lo
             col = lax.broadcasted_iota(jnp.int32, scores.shape, 1)
             scores = jnp.where(col <= row, scores, NEG)
-            high = jnp.max(scores, axis=1, keepdims=True)
-            weights = jnp.exp2((scores - high) * scale).astype(jnp.bfloat16)
+            high = jnp.max(scores, axis=1, keepdims=True) * SCALE
+            weights = jnp.exp2(scores * SCALE - high).astype(jnp.bfloat16)
             summed = f32dot(weights, values[:count])
-            high_ref[span, :] = jnp.broadcast_to(high, (tile, HD))
-            tot_ref[span, :] = summed[:, HD:]
-            sum_ref[span, :] = summed[:, :HD]
+            sum_ref[span, :] = summed[:, :HD] / summed[:, HD:]
+            logs = high + jnp.log2(summed[:, HD:])
+            lane = lax.broadcasted_iota(jnp.int32, logs.shape, 1)
+            before = jnp.where(head == 0, 0.0, log_ref[span, :])
+            log_ref[span, :] = jnp.where(lane == head, logs, before)
 
     column = pl.BlockSpec((rows, HD), lambda h: (0, h))
+    narrow = pl.BlockSpec((rows, HD), lambda h: (0, 0))
     return pl.pallas_call(
         body,
         grid=(heads,),
-        in_specs=[
-            column,
-            column,
-            pl.BlockSpec((rows, HD), lambda h: (0, heads + h)),
-            pl.BlockSpec((rows, HD), lambda h: (0, 0)),
-        ],
-        out_specs=[column, column, column],
-        out_shape=[in_hbm((rows, width), jnp.float32)] * 3,
+        in_specs=[column, column, pl.BlockSpec((rows, HD), lambda h: (0, heads + h)), narrow],
+        out_specs=[column, narrow],
+        out_shape=[in_hbm((rows, width), jnp.float32), in_hbm((rows, HD), jnp.float32)],
         compiler_params=params(),
         cost_estimate=cost(8 * rows * rows * width, 16 * rows * width, rows * rows * heads),
         name="attend_own",
     )(query, *keep_in_hbm(pair, pair, mask))
 
 
-def attend_far(where, query, got, mask, high, total, summed, carried):
+def rows_for(where_ref, parts, tile):
+    def rows_of(ref, cols=slice(None)):
+        spans = [pl.ds(pl.multiple_of(where_ref[p] * tile, tile), tile) for p in parts]
+        return jnp.concatenate([ref[span, cols] for span in spans], axis=0)
+
+    return rows_of
+
+
+def finished(scores, values, own, log):
+    top = jnp.maximum(jnp.max(scores, axis=1, keepdims=True) * SCALE, log)
+    weights = jnp.exp2(scores * SCALE - top).astype(jnp.bfloat16)
+    far = f32dot(weights, values)
+    keep = jnp.exp2(log - top)
+    return ((far[:, :HD] + keep * own) / (far[:, HD:] + keep)).astype(jnp.bfloat16)
+
+
+def attend_first(where, query, got, mask, own, log, parts):
     rows, width = query.shape
     heads = width // HD
     count = got.shape[0]
-    scale = HD ** (-0.5) * LOG2E
-    parts = where.shape[0]
-    tile = rows // parts
-    pairs = ((3, 1), (2, 0))
-
-    def body(where_ref, q_ref, k_ref, v_ref, mask_ref, high_ref, tot_ref, sum_ref, *rest):
-        pieces = len(carried)
+    tile = rows // where.shape[0]
+
+    def body(where_ref, q_ref, got_ref, mask_hbm, own_hbm, log_hbm, out_a, out_b, keys, values, mask, own, log, sems):
         copies = [
-            pltpu.make_async_copy(rest[k], rest[pieces + parts + k], rest[-1].at[k]) for k in range(pieces)
+            pltpu.make_async_copy(src, dst, sems.at[k])
+            for k, (src, dst) in enumerate(((mask_hbm, mask), (own_hbm, own), (log_hbm, log)))
         ]
-        outs = rest[pieces : pieces + parts]
-        keys, values = rest[-3:-1]
-
-        @pl.when(pl.program_id(0) == 1)
-        def _():
-            for copy in copies:
-                copy.start()
-
-        @pl.when(pl.program_id(0) == 0)
-        def _():
-            keys[:, HD:] = one_hot(count, 0)
-            values[:, HD:] = jnp.ones_like(v_ref)
-
-        keys[:, :HD] = k_ref[...]
-        values[:, :HD] = v_ref[...]
-
-        def rows_of(ref, parts_at):
-            spans = [pl.ds(pl.multiple_of(where_ref[p] * tile, tile), tile) for p in parts_at]
-            return jnp.concatenate([ref[span, :] for span in spans], axis=0)
-
-        def scores_at(parts_at):
-            wide = jnp.concatenate([rows_of(q_ref, parts_at), rows_of(mask_ref, parts_at)], axis=1)
-            return scores_of(wide, keys[...])
-
-        later = scores_at(pairs[0])
-        for i, parts_at in enumerate(pairs):
+        for copy in copies:
+            copy.start()
+        hot = one_hot(count, 0)
+        rows_of = rows_for(where_ref, parts, tile)
+
+        def scores_at(h):
+            keys[h, :, :HD] = got_ref[:, h * HD : (h + 1) * HD]
+            keys[h, :, HD:] = hot
+            if h == 0:
+                copies[0].wait()
+            query = rows_of(q_ref, slice(h * HD, (h + 1) * HD))
+            return scores_of(jnp.concatenate([query, rows_of(mask)], axis=1), keys[h])
+
+        later = scores_at(0)
+        for h in range(heads):
             scores = later
-            if i + 1 < len(pairs):
-                later = scores_at(pairs[i + 1])
-            own = rows_of(high_ref, parts_at)
-            top = jnp.maximum(jnp.max(scores, axis=1, keepdims=True), own[:, :1])
-            weights = jnp.exp2((scores - top) * scale).astype(jnp.bfloat16)
-            far = f32dot(weights, values[...])
-            keep = jnp.exp2((own - top) * scale)
-            result = far[:, :HD] + keep * rows_of(sum_ref, parts_at)
-            result = (result / (far[:, HD:] + keep * rows_of(tot_ref, parts_at))).astype(jnp.bfloat16)
-            for k, part in enumerate(parts_at):
-                outs[part][...] = result[k * tile : (k + 1) * tile]
-
-        @pl.when(pl.program_id(0) == heads - 1)
-        def _():
-            for copy in copies:
-                copy.wait()
-
-    column = pl.BlockSpec((rows, HD), lambda h, s: (0, h))
-    return pl.pallas_call(
-        body,
-        grid_spec=pltpu.PrefetchScalarGridSpec(
-            num_scalar_prefetch=1,
-            grid=(heads,),
-            in_specs=[
-                column,
-                pl.BlockSpec((count, HD), lambda h, s: (0, h)),
-                pl.BlockSpec((count, HD), lambda h, s: (0, heads + h)),
-                pl.BlockSpec((rows, HD), lambda h, s: (0, 0)),
-                column,
-                column,
-                column,
-            ]
-            + [HBM] * len(carried),
-            out_specs=[pl.BlockSpec((tile, HD), lambda h, s: (0, h))] * parts + [VMEM] * len(carried),
-            scratch_shapes=[pltpu.VMEM((count, 2 * HD), jnp.bfloat16)] * 2
-            + [pltpu.SemaphoreType.DMA((len(carried),))],
-        ),
-        out_shape=[jax.ShapeDtypeStruct((tile, width), jnp.bfloat16)] * parts
-        + [in_vmem(w.shape, w.dtype) for w in carried],
-        compiler_params=params(),
-        cost_estimate=cost(8 * rows * count * width, 4 * count * width, rows * count * heads),
-        name="attend_far",
-    )(where, query, got, got, *keep_in_hbm(mask, high, total, summed, *carried))
-
-
-def mix(core, attended, w_own, mine, other):
-    rows, width = attended[0].shape
+            values[h, :, :HD] = got_ref[:, (heads + h) * HD : (heads + h + 1) * HD]
+            values[h, :, HD:] = jnp.ones((count, HD), jnp.bfloat16)
+            if h + 1 < heads:
+                later = scores_at(h + 1)
+            if h == 0:
+                copies[1].wait()
+                copies[2].wait()
+            cols = slice(h * HD, (h + 1) * HD)
+            result = finished(scores, values[h], rows_of(own, cols), rows_of(log)[:, h : h + 1])
+            out_a[:, cols] = result[:tile]
+            out_b[:, cols] = result[tile:]
+
+    wides = in_vmem((heads, count, 2 * HD), jnp.bfloat16)
+    return pl.pallas_call(
+        body,
+        in_specs=[SMEM, VMEM, VMEM, HBM, HBM, HBM],
+        out_specs=[VMEM] * 7,
+        out_shape=[in_vmem((tile, width), jnp.bfloat16)] * 2
+        + [wides] * 2
+        + [
+            in_vmem(mask.shape, jnp.bfloat16),
+            in_vmem(own.shape, jnp.float32),
+            in_vmem(log.shape, jnp.float32),
+        ],
+        scratch_shapes=[pltpu.SemaphoreType.DMA((3,))],
+        compiler_params=params(),
+        cost_estimate=cost(4 * rows * count * width, 4 * count * width, rows * count * heads),
+        name="attend_first",
+    )(where, query, got, *keep_in_hbm(mask, own, log))
+
+
+def attend_second(where, query, keys, values, mask, own, log, parts, carried):
+    rows, width = query.shape
+    heads, count, _ = keys.shape
+    tile = rows // where.shape[0]
+    pieces = len(carried)
+
+    def body(where_ref, q_ref, keys_ref, values_ref, mask_ref, own_ref, log_ref, *rest):
+        out_a, out_b = rest[pieces : pieces + 2]
+        copies = [pltpu.make_async_copy(rest[k], rest[pieces + 2 + k], rest[-1].at[k]) for k in range(pieces)]
+        for copy in copies:
+            copy.start()
+        rows_of = rows_for(where_ref, parts, tile)
+
+        def scores_at(h):
+            query = rows_of(q_ref, slice(h * HD, (h + 1) * HD))
+            return scores_of(jnp.concatenate([query, rows_of(mask_ref)], axis=1), keys_ref[h])
+
+        later = scores_at(0)
+        for h in range(heads):
+            scores = later
+            if h + 1 < heads:
+                later = scores_at(h + 1)
+            cols = slice(h * HD, (h + 1) * HD)
+            result = finished(scores, values_ref[h], rows_of(own_ref, cols), rows_of(log_ref)[:, h : h + 1])
+            out_a[:, cols] = result[:tile]
+            out_b[:, cols] = result[tile:]
+        for copy in copies:
+            copy.wait()
+
+    return pl.pallas_call(
+        body,
+        in_specs=[SMEM] + [VMEM] * 6 + [HBM] * pieces,
+        out_specs=[VMEM] * (2 + pieces),
+        out_shape=[in_vmem((tile, width), jnp.bfloat16)] * 2 + [in_vmem(w.shape, w.dtype) for w in carried],
+        scratch_shapes=[pltpu.SemaphoreType.DMA((pieces,))],
+        compiler_params=params(),
+        cost_estimate=cost(4 * rows * count * width, 4 * count * width, rows * count * heads),
+        name="attend_second",
+    )(where, query, keys, values, mask, own, log, *keep_in_hbm(*carried))
+
+
+def mix_near(core, attended, w_own, mine, other):
+    rows = attended[0].shape[0]
     part = mine[0].shape[1]
 
-    def body(core_ref, *rest):
-        own_ref, far_refs, w_ref, pieces = rest[0], rest[1:4], rest[4], (rest[5:11], rest[11:17])
-        out_hbm, out_ref, sems = rest[17:]
-        copies = []
-        for side in range(2):
+    def body(core_ref, own_ref, right_ref, far_ref, w_ref, *rest):
+        out_ref = rest[-1]
+        for side, pieces in enumerate((rest[:4], rest[4:8])):
             base = (core_ref[0] if side == 0 else 1 - core_ref[0]) * 2
             for k in range(2):
                 span = pl.ds(pl.multiple_of((base + k) * part, part), part)
-                total = f32dot(own_ref[...], w_ref[:, span])
-                for g in range(3):
-                    total = total + f32dot(far_refs[g][...], pieces[side][2 * g + k][...])
-                at = 2 * side + k
-                out_ref[at] = total.astype(jnp.bfloat16)
-                copies.append(pltpu.make_async_copy(out_ref.at[at], out_hbm.at[:, span], sems.at[at]))
-                copies[-1].start()
+                total = f32dot(own_ref[...], w_ref[:, span]) + f32dot(right_ref[...], pieces[k][...])
+                out_ref[:, span] = total + f32dot(far_ref[...], pieces[2 + k][...])
+
+    args = (*attended, w_own, *mine, *other)
+    return pl.pallas_call(
+        body,
+        in_specs=[SMEM] + [VMEM] * len(args),
+        out_specs=VMEM,
+        out_shape=in_vmem((rows, 4 * part), jnp.float32),
+        compiler_params=params(),
+        cost_estimate=cost(24 * rows * w_own.shape[0] * part, 24 * w_own.shape[0] * part),
+        name="mix_near",
+    )(core, *args)
+
+
+def mix_last(core, left, mine, other, before):
+    rows = left.shape[0]
+    part = mine[0].shape[1]
+
+    def body(core_ref, left_ref, *rest):
+        before_ref, out_hbm, out_ref, sems = rest[4:]
+        copies = []
+        for at in range(4):
+            base = (core_ref[0] if at < 2 else 1 - core_ref[0]) * 2
+            span = pl.ds(pl.multiple_of((base + at % 2) * part, part), part)
+            out_ref[at] = (before_ref[:, span] + f32dot(left_ref[...], rest[at][...])).astype(jnp.bfloat16)
+            copies.append(pltpu.make_async_copy(out_ref.at[at], out_hbm.at[:, span], sems.at[at]))
+            copies[-1].start()
         for copy in copies:
             copy.wait()
 
-    args = (*attended, w_own, *mine, *other)
-    return pl.pallas_call(
-        body,
-        in_specs=[SMEM] + [VMEM] * len(args),
+    return pl.pallas_call(
+        body,
+        in_specs=[SMEM] + [VMEM] * 6,
         out_specs=HBM,
         out_shape=in_hbm((rows, 4 * part), jnp.bfloat16),
         scratch_shapes=[pltpu.VMEM((4, rows, part), jnp.bfloat16), pltpu.SemaphoreType.DMA((4,))],
         compiler_params=params(),
-        cost_estimate=cost(32 * rows * width * part, 32 * width * part),
-        name="mix",
-    )(core, *args)
+        cost_estimate=cost(8 * rows * left.shape[1] * part, 8 * left.shape[1] * part),
+        name="mix_last",
+    )(core, left, *mine, *other, before)
 
 
 def local(tokens, w_query, w_key, w_value, w_out, chosen):
@@ -465,11 +510,18 @@
     other = tuple(shifted(w, "kv_2", 1) for w in mine)
 
     query = project_query(where, tokens, left, right, top, bottom, w_query)
-    high, totals, summed = attend_own(query, pair, mask, peers * MOST)
-    weights = (w_out, *mine, *other)
-    outs = attend_far(where, query, got.reshape(-1, 2 * width), mask, high, totals, summed, weights)
-    attended = (outs[0], shifted(outs[2], "tp", 1), shifted(outs[1], "tp", -1), shifted(outs[3], "tp", 2))
-    return mix(core, attended, outs[4], outs[5:11], outs[11:])
+    own, log = attend_own(query, pair, mask, peers * MOST)
+    to_far, to_left, keys, values, mask, own, log = attend_first(
+        where, query, got.reshape(-1, 2 * width), mask, own, log, (3, 1)
+    )
+    far = shifted(to_far, "tp", 2)
+    right = shifted(to_left, "tp", -1)
+    carried = (w_out, *mine, *other)
+    to_right, mid, w_own, *pieces = attend_second(where, query, keys, values, mask, own, log, (2, 0), carried)
+    left = shifted(to_right, "tp", 1)
+    mine, other = pieces[:6], pieces[6:]
+    before = mix_near(core, (mid, right, far), w_own, mine[2:], other[2:])
+    return mix_last(core, left, mine[:2], other[:2], before)
 
 
 def solution(mesh):

time: 109 us -> 109 us (level)
  Pallas kernels: 27.4 us -> 29.6 us
  starting transfers between devices: 32.3 us -> 30.5 us
  local copies, waits for them, and re-layouts: 5.41 us -> 3.67 us
  waiting for transfers between devices: 42.8 us -> 44.1 us
    pallas_call x2 -> x4, Pallas kernels: 9.53 us -> 11.9 us  [the longest x1 5.18 us: attend_second(): pl.pallas_call(body, in_specs=[SMEM] + [VMEM] * 6 + [HBM] * pieces, out_s...]
    all_to_all x1, waiting for transfers between devices: 0.34 us -> 2.18 us  [local(): got = lax.all_to_all(send, KV, split_axis=0, concat_axis=0, tiled=True)]
    unnamed x30 -> x12, local copies, waits for them, and re-layouts: 3.97 us -> 2.22 us
    ppermute x19, starting transfers between devices: 17.6 us -> 15.9 us  [shifted(): lax.ppermute(array, axis, [(i, (i + by) % count) for i in range(count)])]
  transfers between devices with their start and end apart: 21 -> 21, of which waited for: 12 -> 11; matrix products, arithmetic and copies ran while one was open for 0% -> 0% of each run, Pallas kernels for 13% -> 23%
where the time goes in v2:
time: 109 us; the launch traced here: 108 us
  waiting for transfers between devices  44.1 us (40%)
  starting transfers between devices  30.5 us (28%)
  Pallas kernels  29.6 us (27%)
  local copies, waits for them, and re-layouts  3.67 us (3%)
    ppermute x19, waiting for transfers between devices, shifted(): lax.ppermute(array, axis, [(i, (i + by) % count) for i in range(count)])  40.6 us
    ppermute x19, starting transfers between devices, shifted(): lax.ppermute(array, axis, [(i, (i + by) % count) for i in range(count)])  15.9 us
    all_to_all x1, starting transfers between devices, local(): asked = lax.all_to_all(request, KV, 0, 0, tiled=True)  8.33 us
    all_to_all x1, starting transfers between devices, local(): got = lax.all_to_all(send, KV, split_axis=0, concat_axis=0, tiled=True)  6.27 us
    pallas_call x1, Pallas kernels, attend_second(): pl.pallas_call(body, in_specs=[SMEM] + [VMEM] * 6 + [HBM] * pieces, out_s...  5.18 us
    pallas_call x1, Pallas kernels, project_near(): pl.pallas_call(body, in_specs=[SMEM, SMEM, HBM, VMEM, VMEM, HBM, HBM, HBM...  4.59 us
    pallas_call x1, Pallas kernels, attend_first(): pl.pallas_call(body, in_specs=[SMEM, VMEM, VMEM, HBM, HBM, HBM], out_spec...  4.58 us
    pallas_call x1, Pallas kernels, attend_own(): pl.pallas_call(body, grid=(heads,), in_specs=[column, column, pl.BlockSpe...  4.57 us
  transfers between devices with their start and end apart: 21, of which 11 were waited for; matrix products, arithmetic and copies ran while one was open for 0% of the time, Pallas kernels for 23%

profile of v2, /device:TPU:0, one launch (start us, length us, event | category | flops | bytes accessed | tf_op | source)
XLA Modules:
  0.0 108.3 jit_solution(7393719241476263845)
XLA Ops:
  0.1 2.9 %collective-permute-start.1 = (bf16[512,512]{1,0:T(8,128)(2,1)}, bf16[512,512]{1,0:T(8,128)(2,1)S(1)}, u32[]{:S(2)}, u32[]{:S(2)}) collective-permute-start(bf16[512,512]{1,0:T(8,128)(2,1)} %o_ref), channel_id=1, source_target_pairs={{0,3},{1,0},{2,1},{3,2},{4,7},{5,4},{6,5},{7,6},{8,11},{9,8},{10,9... | collective-permute-start | bytes 1572872 | tf_op jit(solution)/shard_map/ppermute | solution.py:49
  3.0 0.7 copy-done
  3.7 1.0 plan.1
  4.6 9.8 %collective-permute-done.1.r_ref = bf16[512,512]{1,0:T(8,128)(2,1)S(1)} collective-permute-done((bf16[512,512]{1,0:T(8,128)(2,1)}, bf16[512,512]{1,0:T(8,128)(2,1)S(1)}, u32[]{:S(2)}, u32[]{:S(2)}) %collective-permute-start.1) | collective-permute-done | bytes 524320 | tf_op jit(solution)/shard_map/ppermute | solution.py:49
  14.5 3.3 %collective-permute-done.l_ref = bf16[512,512]{1,0:T(8,128)(2,1)S(1)} collective-permute-done((bf16[512,512]{1,0:T(8,128)(2,1)}, bf16[512,512]{1,0:T(8,128)(2,1)S(1)}, u32[]{:S(2)}, u32[]{:S(2)}) %collective-permute-start) | collective-permute-done | bytes 524320 | tf_op jit(solution)/shard_map/ppermute | solution.py:49
  17.8 0.7 slice.6
  18.5 0.7 slice.7
  19.5 1.7 %collective-permute-start.2 = (bf16[256,512]{1,0:T(8,128)(2,1)}, bf16[256,512]{1,0:T(8,128)(2,1)}, u32[]{:S(2)}, u32[]{:S(2)}) collective-permute-start(bf16[256,512]{1,0:T(8,128)(2,1)} %slice.6), channel_id=1, source_target_pairs={{0,1},{1,2},{2,3},{3,0},{4,5},{5,6},{6,7},{7,4},{8,9},{9,10},{10,1... | collective-permute-start | bytes 786440 | tf_op jit(solution)/shard_map/ppermute | solution.py:49
  21.2 8.3 %all-to-all-start = ((s32[32,1,128]{2,1,0:T(1,128)}), s32[32,1,128]{2,1,0:T(1,128)S(1)}, u32[]{:S(2)}, u32[]{:S(2)}) async-start(s32[32,1,128]{2,1,0:T(1,128)} %bitcast.13), calls=%async_computation | async-start | bytes 32768 | tf_op jit(solution)/shard_map/all_to_all | solution.py:491
  29.6 4.6 %project_near.1 = (f32[512,768]{1,0:T(8,128)S(1)}, bf16[512,384]{1,0:T(8,128)(2,1)S(1)}, bf16[512,384]{1,0:T(8,128)(2,1)S(1)}, bf16[512,512]{1,0:T(8,128)(2,1)},...) custom-call(s32[4]{0:T(128)S(1)} %pad_add_fusion.where_ref, ...), custom_call_target="tpu_custom_call" | custom-call | flops 1207959552 | bytes 3932160 | tf_op jit(solution)/shard_map/project_near/pallas_call | solution.py:89
  34.2 0.7 copy-done.1
  34.9 0.8 copy-done.3
  35.7 1.3 %all-to-all-done = s32[32,1,128]{2,1,0:T(1,128)S(1)} async-done(((s32[32,1,128]{2,1,0:T(1,128)}), s32[32,1,128]{2,1,0:T(1,128)S(1)}, u32[]{:S(2)}, u32[]{:S(2)}) %all-to-all-start) | async-done | bytes 16416 | tf_op jit(solution)/shard_map/all_to_all | solution.py:491
  37.0 3.8 %project_last.1 = (bf16[512,768]{1,0:T(8,128)(2,1)}, bf16[64,32,768]{2,1,0:T(8,128)(2,1)}, bf16[256,512]{1,0:T(8,128)(2,1)}, bf16[256,512]{1,0:T(8,128)(2,1)}) custom-call(s32[32,128]{1,0:T(8,128)S(1)} %bitcast.12, bf16[256,512]{1,0:T(8,128)(2,1)} %collective-permute-done.2.t_ref, bf16[256,512]{1,0:T(8,128)(2,1)} %collective-permute-done.3.b_ref, ...), custom_call_target="tpu_custom_call" | custom-call | flops 402653184 | bytes 2359296 | tf_op jit(solution)/shard_map/project_last/pallas_call | solution.py:149
  40.8 6.3 %all-to-all-start.1 = ((bf16[64,32,768]{2,1,0:T(8,128)(2,1)}), bf16[64,32,768]{2,1,0:T(8,128)(2,1)S(1)}, u32[]{:S(2)}, u32[]{:S(2)}) async-start(bf16[64,32,768]{2,1,0:T(8,128)(2,1)} %get-tuple-element.70), calls=%async_computation.1 | async-start | bytes 6291456 | tf_op jit(solution)/shard_map/all_to_all | solution.py:501
  47.1 1.6 %collective-permute-start.6 = (bf16[384,512]{1,0:T(8,128)(2,1)}, bf16[384,512]{1,0:T(8,128)(2,1)S(1)}, u32[]{:S(2)}, u32[]{:S(2)}) collective-permute-start(bf16[384,512]{1,0:T(8,128)(2,1)} %copy-done.3), channel_id=1, source_target_pairs={{0,3},{1,0},{2,1},{3,2},{4,7},{5,4},{6,5},{7,6},{8,11},{9,8},{10,9... | collective-permute-start | bytes 1179656 | tf_op jit(solution)/shard_map/ppermute | solution.py:49
  49.2 2.7 %collective-permute-start.7 = (bf16[384,512]{1,0:T(8,128)(2,1)S(1)}, bf16[384,512]{1,0:T(8,128)(2,1)}, u32[]{:S(2)}, u32[]{:S(2)}) collective-permute-start(bf16[384,512]{1,0:T(8,128)(2,1)S(1)} %copy-done.2), channel_id=1, source_target_pairs={{0,3},{1,0},{2,1},{3,2},{4,7},{5,4},{6,5},{7,6},{8,11},{9,8},{10,9... | collective-permute-start | bytes 1179656 | tf_op jit(solution)/shard_map/ppermute | solution.py:49
  51.9 7.5 %collective-permute-done.6.rest_3_ = bf16[384,512]{1,0:T(8,128)(2,1)S(1)} collective-permute-done((bf16[384,512]{1,0:T(8,128)(2,1)}, bf16[384,512]{1,0:T(8,128)(2,1)S(1)}, u32[]{:S(2)}, u32[]{:S(2)}) %collective-permute-start.6) | collective-permute-done | bytes 393248 | tf_op jit(solution)/shard_map/ppermute | solution.py:49
  59.4 2.8 %collective-permute-done.4.rest_1_ = bf16[384,512]{1,0:T(8,128)(2,1)} collective-permute-done((bf16[384,512]{1,0:T(8,128)(2,1)}, bf16[384,512]{1,0:T(8,128)(2,1)}, u32[]{:S(2)}, u32[]{:S(2)}) %collective-permute-start.4) | collective-permute-done | bytes 393248 | tf_op jit(solution)/shard_map/ppermute | solution.py:49
  62.2 5.0 %collective-permute-done.7.rest_4_ = bf16[384,512]{1,0:T(8,128)(2,1)} collective-permute-done((bf16[384,512]{1,0:T(8,128)(2,1)S(1)}, bf16[384,512]{1,0:T(8,128)(2,1)}, u32[]{:S(2)}, u32[]{:S(2)}) %collective-permute-start.7) | collective-permute-done | bytes 393248 | tf_op jit(solution)/shard_map/ppermute | solution.py:49
  67.2 2.7 %collective-permute-start.9 = (bf16[384,512]{1,0:T(8,128)(2,1)}, bf16[384,512]{1,0:T(8,128)(2,1)}, u32[]{:S(2)}, u32[]{:S(2)}) collective-permute-start(bf16[384,512]{1,0:T(8,128)(2,1)} %collective-permute-done.7.rest_4_), channel_id=1, source_target_pairs={{0,3},{1,0},{2,1},{3,2},{4,7},{5,4},{6,5},{7,6},{8,11},{9,8},{10,9... | collective-permute-start | bytes 1179656 | tf_op jit(solution)/shard_map/ppermute | solution.py:49
  69.9 0.7 collective-permute-done.5.rest_2_
  71.1 6.9 %collective-permute-done.8.rest_5_ = bf16[384,512]{1,0:T(8,128)(2,1)} collective-permute-done((bf16[384,512]{1,0:T(8,128)(2,1)}, bf16[384,512]{1,0:T(8,128)(2,1)}, u32[]{:S(2)}, u32[]{:S(2)}) %collective-permute-start.8) | collective-permute-done | bytes 393248 | tf_op jit(solution)/shard_map/ppermute | solution.py:49
  78.6 3.8 %project_query.1.q_ref = bf16[512,384]{1,0:T(8,128)(2,1)S(1)} custom-call(s32[4]{0:T(128)S(1)} %pad_add_fusion.where_ref, bf16[512,512]{1,0:T(8,128)(2,1)} %o_ref, bf16[512,512]{1,0:T(8,128)(2,1)} %get-tuple-element.60.l_ref, bf16[512,512]{1,0:T(8,128)(2,1)} %get-tuple-element.61.r_ref, bf16[256,512]{1,0:T(8,128)(2,1)} %get-tuple-element.65.t_ref, ...), custom_call_target="tpu_custom_call" | custom-call | flops 805306368 | bytes 3145728 | tf_op jit(solution)/shard_map/project_query/pallas_call | solution.py:189
  82.3 4.6 %attend_own.1 = (f32[512,384]{1,0:T(8,128)}, f32[512,128]{1,0:T(8,128)}) custom-call(bf16[512,384]{1,0:T(8,128)(2,1)S(1)} %project_query.1.q_ref, bf16[512,768]{1,0:T(8,128)(2,1)} %get-tuple-element.72.k_ref.v_ref, bf16[512,768]{1,0:T(8,128)(2,1)} %get-tuple-element.72.k_ref.v_ref, bf16[512,128]{1,0:T(8,128)(2,1)} %get-tuple-element.71.mask_ref.mask_hbm), custom_call_target="tpu_custom_call" | custom-call | flops 805306368 | bytes 3145728 | tf_op jit(solution)/shard_map/attend_own/pallas_call | solution.py:296
  86.9 2.2 %all-to-all-done.1 = bf16[64,32,768]{2,1,0:T(8,128)(2,1)S(1)} async-done(((bf16[64,32,768]{2,1,0:T(8,128)(2,1)}), bf16[64,32,768]{2,1,0:T(8,128)(2,1)S(1)}, u32[]{:S(2)}, u32[]{:S(2)}) %all-to-all-start.1) | async-done | bytes 3145760 | tf_op jit(solution)/shard_map/all_to_all | solution.py:501
  89.1 4.6 %attend_first.1 = (bf16[128,384]{1,0:T(8,128)(2,1)S(1)}, bf16[128,384]{1,0:T(8,128)(2,1)S(1)}, bf16[3,2048,256]{2,1,0:T(8,128)(2,1)S(1)}, bf16[3,2048,256]{2,1,0...) custom-call(s32[4]{0:T(128)S(1)} %pad_add_fusion.where_ref, ...), custom_call_target="tpu_custom_call" | custom-call | flops 1610612736 | bytes 3145728 | tf_op jit(solution)/shard_map/attend_first/pallas_call | solution.py:364
  93.7 1.6 %collective-permute-start.17 = (bf16[128,384]{1,0:T(8,128)(2,1)S(1)}, bf16[128,384]{1,0:T(8,128)(2,1)S(1)}, u32[]{:S(2)}, u32[]{:S(2)}) collective-permute-start(bf16[128,384]{1,0:T(8,128)(2,1)S(1)} %get-tuple-element.88), channel_id=1, source_target_pairs={{0,3},{1,0},{2,1},{3,2},{4,7},{5,4},{6,5},{7,6},{8,11},{9,8},{10,9... | collective-permute-start | bytes 294920 | tf_op jit(solution)/shard_map/ppermute | solution.py:49
  95.9 5.2 %attend_second.1 = (bf16[128,384]{1,0:T(8,128)(2,1)S(1)}, bf16[128,384]{1,0:T(8,128)(2,1)S(1)}, bf16[384,2048]{1,0:T(8,128)(2,1)S(1)}, bf16[384,512]{1,0:T(8,128...) custom-call(s32[4]{0:T(128)S(1)} %pad_add_fusion.where_ref, ...), custom_call_target="tpu_custom_call" | custom-call | flops 1610612736 | bytes 3145728 | tf_op jit(solution)/shard_map/attend_second/pallas_call | solution.py:411
  101.5 1.0 mix_near.1.rest_4_
  102.5 4.4 %collective-permute-done.16.left_ref = bf16[128,384]{1,0:T(8,128)(2,1)S(1)} collective-permute-done((bf16[128,384]{1,0:T(8,128)(2,1)S(1)}, bf16[128,384]{1,0:T(8,128)(2,1)S(1)}, u32[]{:S(2)}, u32[]{:S(2)}) %collective-permute-start.16) | collective-permute-done | bytes 98336 | tf_op jit(solution)/shard_map/ppermute | solution.py:49
  106.9 1.2 %mix_last.1 = bf16[128,2048]{1,0:T(8,128)(2,1)} custom-call(s32[1]{0:T(128)} %bitcast.5.core_ref, bf16[128,384]{1,0:T(8,128)(2,1)S(1)} %collective-permute-done.16.left_ref, bf16[384,512]{1,0:T(8,128)(2,1)S(1)} %get-tuple-element.83.rest_0_, bf16[384,512]{1,0:T(8,128)(2,1)S(1)} %get-tuple-element.84.rest_1_, bf16[384,512]{1,0:T(8,128)(2,1)S(1)} %get-tuple-element.85.rest_2_, ...), custom_call_target="tpu_custom_call" | custom-call | flops 201326592 | bytes 1572864 | tf_op jit(solution)/shard_map/mix_last/pallas_call | solution.py:464
  (34 shorter events, 3.0 us)
Async XLA Ops:
  0.1 14.4 %collective-permute-start.1 = (bf16[512,512]{1,0:T(8,128)(2,1)}, bf16[512,512]{1,0:T(8,128)(2,1)S(1)}, u32[]{:S(2)}, u32[]{:S(2)}) collective-permute-start(bf16[512,512]{1,0:T(8,128)(2,1)} %o_ref), channel_id=1, source_target_pairs={{0,3},{1,0},{2,1},{3,2},{4,7},{5,4},{6,5},{7,6},{8,11},{9,8},{10,9... | collective-permute-start | bytes 1572872 | tf_op jit(solution)/shard_map/ppermute | solution.py:49
  3.0 14.8 %collective-permute-start = (bf16[512,512]{1,0:T(8,128)(2,1)}, bf16[512,512]{1,0:T(8,128)(2,1)S(1)}, u32[]{:S(2)}, u32[]{:S(2)}) collective-permute-start(bf16[512,512]{1,0:T(8,128)(2,1)} %o_ref), channel_id=1, source_target_pairs={{0,1},{1,2},{2,3},{3,0},{4,5},{5,6},{6,7},{7,4},{8,9},{9,10},{10,1... | collective-permute-start | bytes 1572872 | tf_op jit(solution)/shard_map/ppermute | solution.py:49
  3.0 0.7 copy-start
  19.2 17.7 %collective-permute-start.3 = (bf16[256,512]{1,0:T(8,128)(2,1)}, bf16[256,512]{1,0:T(8,128)(2,1)}, u32[]{:S(2)}, u32[]{:S(2)}) collective-permute-start(bf16[256,512]{1,0:T(8,128)(2,1)} %slice.7), channel_id=1, source_target_pairs={{0,3},{1,0},{2,1},{3,2},{4,7},{5,4},{6,5},{7,6},{8,11},{9,8},{10,9... | collective-permute-start | bytes 786440 | tf_op jit(solution)/shard_map/ppermute | solution.py:49
  19.5 17.5 %collective-permute-start.2 = (bf16[256,512]{1,0:T(8,128)(2,1)}, bf16[256,512]{1,0:T(8,128)(2,1)}, u32[]{:S(2)}, u32[]{:S(2)}) collective-permute-start(bf16[256,512]{1,0:T(8,128)(2,1)} %slice.6), channel_id=1, source_target_pairs={{0,1},{1,2},{2,3},{3,0},{4,5},{5,6},{6,7},{7,4},{8,9},{9,10},{10,1... | collective-permute-start | bytes 786440 | tf_op jit(solution)/shard_map/ppermute | solution.py:49
  21.2 15.7 %all-to-all-start = ((s32[32,1,128]{2,1,0:T(1,128)}), s32[32,1,128]{2,1,0:T(1,128)S(1)}, u32[]{:S(2)}, u32[]{:S(2)}) async-start(s32[32,1,128]{2,1,0:T(1,128)} %bitcast.13), calls=%async_computation | async-start | bytes 32768 | tf_op jit(solution)/shard_map/all_to_all | solution.py:491
  34.2 0.8 copy-start.1
  34.9 0.8 copy-start.3
  40.8 8.4 %copy-start.2 = (bf16[384,512]{1,0:T(8,128)(2,1)S(1)}, bf16[384,512]{1,0:T(8,128)(2,1)}, u32[]{:S(2)}) copy-start(bf16[384,512]{1,0:T(8,128)(2,1)} %copy-done.1) | copy-start | bytes 1179652
  40.8 48.3 %all-to-all-start.1 = ((bf16[64,32,768]{2,1,0:T(8,128)(2,1)}), bf16[64,32,768]{2,1,0:T(8,128)(2,1)S(1)}, u32[]{:S(2)}, u32[]{:S(2)}) async-start(bf16[64,32,768]{2,1,0:T(8,128)(2,1)} %get-tuple-element.70), calls=%async_computation.1 | async-start | bytes 6291456 | tf_op jit(solution)/shard_map/all_to_all | solution.py:501
  47.1 12.3 %collective-permute-start.6 = (bf16[384,512]{1,0:T(8,128)(2,1)}, bf16[384,512]{1,0:T(8,128)(2,1)S(1)}, u32[]{:S(2)}, u32[]{:S(2)}) collective-permute-start(bf16[384,512]{1,0:T(8,128)(2,1)} %copy-done.3), channel_id=1, source_target_pairs={{0,3},{1,0},{2,1},{3,2},{4,7},{5,4},{6,5},{7,6},{8,11},{9,8},{10,9... | collective-permute-start | bytes 1179656 | tf_op jit(solution)/shard_map/ppermute | solution.py:49
  48.7 13.5 %collective-permute-start.4 = (bf16[384,512]{1,0:T(8,128)(2,1)}, bf16[384,512]{1,0:T(8,128)(2,1)}, u32[]{:S(2)}, u32[]{:S(2)}) collective-permute-start(bf16[384,512]{1,0:T(8,128)(2,1)} %copy-done.3), channel_id=1, source_target_pairs={{0,1},{1,2},{2,3},{3,0},{4,5},{5,6},{6,7},{7,4},{8,9},{9,10},{10,1... | collective-permute-start | bytes 1179656 | tf_op jit(solution)/shard_map/ppermute | solution.py:49
  49.2 18.0 %collective-permute-start.7 = (bf16[384,512]{1,0:T(8,128)(2,1)S(1)}, bf16[384,512]{1,0:T(8,128)(2,1)}, u32[]{:S(2)}, u32[]{:S(2)}) collective-permute-start(bf16[384,512]{1,0:T(8,128)(2,1)S(1)} %copy-done.2), channel_id=1, source_target_pairs={{0,3},{1,0},{2,1},{3,2},{4,7},{5,4},{6,5},{7,6},{8,11},{9,8},{10,9... | collective-permute-start | bytes 1179656 | tf_op jit(solution)/shard_map/ppermute | solution.py:49
  51.9 18.7 %collective-permute-start.5 = (bf16[384,512]{1,0:T(8,128)(2,1)S(1)}, bf16[384,512]{1,0:T(8,128)(2,1)}, u32[]{:S(2)}, u32[]{:S(2)}) collective-permute-start(bf16[384,512]{1,0:T(8,128)(2,1)S(1)} %copy-done.2), channel_id=1, source_target_pairs={{0,1},{1,2},{2,3},{3,0},{4,5},{5,6},{6,7},{7,4},{8,9},{9,10},{10,1... | collective-permute-start | bytes 1179656 | tf_op jit(solution)/shard_map/ppermute | solution.py:49
  59.4 19.2 %copy-start.4 = (bf16[384,512]{1,0:T(8,128)(2,1)}, bf16[384,512]{1,0:T(8,128)(2,1)S(1)}, u32[]{:S(2)}) copy-start(bf16[384,512]{1,0:T(8,128)(2,1)S(1)} %collective-permute-done.6.rest_3_) | copy-start | bytes 1179652
  59.4 11.2 %collective-permute-start.12 = (bf16[384,512]{1,0:T(8,128)(2,1)S(1)}, bf16[384,512]{1,0:T(8,128)(2,1)S(1)}, u32[]{:S(2)}, u32[]{:S(2)}) collective-permute-start(bf16[384,512]{1,0:T(8,128)(2,1)S(1)} %collective-permute-done.6.rest_3_), channel_id=1, source_target_pairs={{0,4},{4,0},{1,5},{5,1},{2,6},{6,2},{3,7},{7,3},{8,12},{12,8},{9,1... | collective-permute-start | bytes 1179656 | tf_op jit(solution)/shard_map/ppermute | solution.py:49
  62.2 15.9 %collective-permute-start.8 = (bf16[384,512]{1,0:T(8,128)(2,1)}, bf16[384,512]{1,0:T(8,128)(2,1)}, u32[]{:S(2)}, u32[]{:S(2)}) collective-permute-start(bf16[384,512]{1,0:T(8,128)(2,1)} %collective-permute-done.4.rest_1_), channel_id=1, source_target_pairs={{0,1},{1,2},{2,3},{3,0},{4,5},{5,6},{6,7},{7,4},{8,9},{9,10},{10,1... | collective-permute-start | bytes 1179656 | tf_op jit(solution)/shard_map/ppermute | solution.py:49
  67.2 11.0 %collective-permute-start.9 = (bf16[384,512]{1,0:T(8,128)(2,1)}, bf16[384,512]{1,0:T(8,128)(2,1)}, u32[]{:S(2)}, u32[]{:S(2)}) collective-permute-start(bf16[384,512]{1,0:T(8,128)(2,1)} %collective-permute-done.7.rest_4_), channel_id=1, source_target_pairs={{0,3},{1,0},{2,1},{3,2},{4,7},{5,4},{6,5},{7,6},{8,11},{9,8},{10,9... | collective-permute-start | bytes 1179656 | tf_op jit(solution)/shard_map/ppermute | solution.py:49
  69.9 23.8 %collective-permute-start.10 = (bf16[384,512]{1,0:T(8,128)(2,1)}, bf16[384,512]{1,0:T(8,128)(2,1)}, u32[]{:S(2)}, u32[]{:S(2)}) collective-permute-start(bf16[384,512]{1,0:T(8,128)(2,1)} %collective-permute-done.4.rest_1_), channel_id=1, source_target_pairs={{0,4},{4,0},{1,5},{5,1},{2,6},{6,2},{3,7},{7,3},{8,12},{12,8},{9,1... | collective-permute-start | bytes 1179656 | tf_op jit(solution)/shard_map/ppermute | solution.py:49
  70.6 24.7 %collective-permute-start.13 = (bf16[384,512]{1,0:T(8,128)(2,1)}, bf16[384,512]{1,0:T(8,128)(2,1)}, u32[]{:S(2)}, u32[]{:S(2)}) collective-permute-start(bf16[384,512]{1,0:T(8,128)(2,1)} %collective-permute-done.7.rest_4_), channel_id=1, source_target_pairs={{0,4},{4,0},{1,5},{5,1},{2,6},{6,2},{3,7},{7,3},{8,12},{12,8},{9,1... | collective-permute-start | bytes 1179656 | tf_op jit(solution)/shard_map/ppermute | solution.py:49
  70.6 8.0 %copy-start.5 = (bf16[384,512]{1,0:T(8,128)(2,1)}, bf16[384,512]{1,0:T(8,128)(2,1)S(1)}, u32[]{:S(2)}) copy-start(bf16[384,512]{1,0:T(8,128)(2,1)S(1)} %collective-permute-done.12.rest_9_) | copy-start | bytes 1179652
  70.6 25.2 %collective-permute-start.11 = (bf16[384,512]{1,0:T(8,128)(2,1)}, bf16[384,512]{1,0:T(8,128)(2,1)}, u32[]{:S(2)}, u32[]{:S(2)}) collective-permute-start(bf16[384,512]{1,0:T(8,128)(2,1)} %collective-permute-done.5.rest_2_), channel_id=1, source_target_pairs={{0,4},{4,0},{1,5},{5,1},{2,6},{6,2},{3,7},{7,3},{8,12},{12,8},{9,1... | collective-permute-start | bytes 1179656 | tf_op jit(solution)/shard_map/ppermute | solution.py:49
  78.1 17.8 %collective-permute-start.14 = (bf16[384,512]{1,0:T(8,128)(2,1)}, bf16[384,512]{1,0:T(8,128)(2,1)}, u32[]{:S(2)}, u32[]{:S(2)}) collective-permute-start(bf16[384,512]{1,0:T(8,128)(2,1)} %collective-permute-done.8.rest_5_), channel_id=1, source_target_pairs={{0,4},{4,0},{1,5},{5,1},{2,6},{6,2},{3,7},{7,3},{8,12},{12,8},{9,1... | collective-permute-start | bytes 1179656 | tf_op jit(solution)/shard_map/ppermute | solution.py:49
  78.2 17.7 %collective-permute-start.15 = (bf16[384,512]{1,0:T(8,128)(2,1)}, bf16[384,512]{1,0:T(8,128)(2,1)}, u32[]{:S(2)}, u32[]{:S(2)}) collective-permute-start(bf16[384,512]{1,0:T(8,128)(2,1)} %collective-permute-done.9.rest_6_), channel_id=1, source_target_pairs={{0,4},{4,0},{1,5},{5,1},{2,6},{6,2},{3,7},{7,3},{8,12},{12,8},{9,1... | collective-permute-start | bytes 1179656 | tf_op jit(solution)/shard_map/ppermute | solution.py:49
  93.7 7.8 %collective-permute-start.17 = (bf16[128,384]{1,0:T(8,128)(2,1)S(1)}, bf16[128,384]{1,0:T(8,128)(2,1)S(1)}, u32[]{:S(2)}, u32[]{:S(2)}) collective-permute-start(bf16[128,384]{1,0:T(8,128)(2,1)S(1)} %get-tuple-element.88), channel_id=1, source_target_pairs={{0,3},{1,0},{2,1},{3,2},{4,7},{5,4},{6,5},{7,6},{8,11},{9,8},{10,9... | collective-permute-start | bytes 294920 | tf_op jit(solution)/shard_map/ppermute | solution.py:49
  95.3 6.2 %collective-permute-start.18 = (bf16[128,384]{1,0:T(8,128)(2,1)S(1)}, bf16[128,384]{1,0:T(8,128)(2,1)S(1)}, u32[]{:S(2)}, u32[]{:S(2)}) collective-permute-start(bf16[128,384]{1,0:T(8,128)(2,1)S(1)} %get-tuple-element.89), channel_id=1, source_target_pairs={{0,2},{1,3},{2,0},{3,1},{4,6},{5,7},{6,4},{7,5},{8,10},{9,11},{10,... | collective-permute-start | bytes 294920 | tf_op jit(solution)/shard_map/ppermute | solution.py:49
  101.0 5.9 %collective-permute-start.16 = (bf16[128,384]{1,0:T(8,128)(2,1)S(1)}, bf16[128,384]{1,0:T(8,128)(2,1)S(1)}, u32[]{:S(2)}, u32[]{:S(2)}) collective-permute-start(bf16[128,384]{1,0:T(8,128)(2,1)S(1)} %get-tuple-element.82), channel_id=1, source_target_pairs={{0,1},{1,2},{2,3},{3,0},{4,5},{5,6},{6,7},{7,4},{8,9},{9,10},{10,1... | collective-permute-start | bytes 294920 | tf_op jit(solution)/shard_map/ppermute | solution.py:49

commit v3 on v2

--- a/solution.py
+++ b/solution.py
@@ -321,13 +321,16 @@
     return ((far[:, :HD] + keep * own) / (far[:, HD:] + keep)).astype(jnp.bfloat16)
 
 
-def attend_first(where, query, got, mask, own, log, parts):
+def attend_first(where, query, got, mask, own, log, groups):
     rows, width = query.shape
     heads = width // HD
     count = got.shape[0]
     tile = rows // where.shape[0]
-
-    def body(where_ref, q_ref, got_ref, mask_hbm, own_hbm, log_hbm, out_a, out_b, keys, values, mask, own, log, sems):
+    places = [part for group in groups for part in group]
+    outs = len(places)
+
+    def body(where_ref, q_ref, got_ref, mask_hbm, own_hbm, log_hbm, *rest):
+        keys, values, mask, own, log, sems = rest[outs:]
         copies = [
             pltpu.make_async_copy(src, dst, sems.at[k])
             for k, (src, dst) in enumerate(((mask_hbm, mask), (own_hbm, own), (log_hbm, log)))
@@ -335,37 +338,42 @@
         for copy in copies:
             copy.start()
         hot = one_hot(count, 0)
-        rows_of = rows_for(where_ref, parts, tile)
-
-        def scores_at(h):
-            keys[h, :, :HD] = got_ref[:, h * HD : (h + 1) * HD]
-            keys[h, :, HD:] = hot
-            if h == 0:
+        steps = [(h, group) for h in range(heads) for group in groups]
+
+        def scores_at(i):
+            h, group = steps[i]
+            if i % len(groups) == 0:
+                keys[h, :, :HD] = got_ref[:, h * HD : (h + 1) * HD]
+                keys[h, :, HD:] = hot
+            if i == 0:
                 copies[0].wait()
+            rows_of = rows_for(where_ref, group, tile)
             query = rows_of(q_ref, slice(h * HD, (h + 1) * HD))
             return scores_of(jnp.concatenate([query, rows_of(mask)], axis=1), keys[h])
 
         later = scores_at(0)
-        for h in range(heads):
+        for i, (h, group) in enumerate(steps):
             scores = later
-            values[h, :, :HD] = got_ref[:, (heads + h) * HD : (heads + h + 1) * HD]
-            values[h, :, HD:] = jnp.ones((count, HD), jnp.bfloat16)
-            if h + 1 < heads:
-                later = scores_at(h + 1)
-            if h == 0:
+            if i % len(groups) == 0:
+                values[h, :, :HD] = got_ref[:, (heads + h) * HD : (heads + h + 1) * HD]
+                values[h, :, HD:] = jnp.ones((count, HD), jnp.bfloat16)
+            if i + 1 < len(steps):
+                later = scores_at(i + 1)
+            if i == 0:
                 copies[1].wait()
                 copies[2].wait()
             cols = slice(h * HD, (h + 1) * HD)
+            rows_of = rows_for(where_ref, group, tile)
             result = finished(scores, values[h], rows_of(own, cols), rows_of(log)[:, h : h + 1])
-            out_a[:, cols] = result[:tile]
-            out_b[:, cols] = result[tile:]
+            for k, part in enumerate(group):
+                rest[places.index(part)][:, cols] = result[k * tile : (k + 1) * tile]
 
     wides = in_vmem((heads, count, 2 * HD), jnp.bfloat16)
     return pl.pallas_call(
         body,
         in_specs=[SMEM, VMEM, VMEM, HBM, HBM, HBM],
-        out_specs=[VMEM] * 7,
-        out_shape=[in_vmem((tile, width), jnp.bfloat16)] * 2
+        out_specs=[VMEM] * (outs + 5),
+        out_shape=[in_vmem((tile, width), jnp.bfloat16)] * outs
         + [wides] * 2
         + [
             in_vmem(mask.shape, jnp.bfloat16),
@@ -374,23 +382,23 @@
         ],
         scratch_shapes=[pltpu.SemaphoreType.DMA((3,))],
         compiler_params=params(),
-        cost_estimate=cost(4 * rows * count * width, 4 * count * width, rows * count * heads),
+        cost_estimate=cost(6 * rows * count * width, 4 * count * width, rows * count * heads),
         name="attend_first",
     )(where, query, got, *keep_in_hbm(mask, own, log))
 
 
-def attend_second(where, query, keys, values, mask, own, log, parts, carried):
+def attend_second(where, query, keys, values, mask, own, log, carried):
     rows, width = query.shape
     heads, count, _ = keys.shape
     tile = rows // where.shape[0]
     pieces = len(carried)
 
     def body(where_ref, q_ref, keys_ref, values_ref, mask_ref, own_ref, log_ref, *rest):
-        out_a, out_b = rest[pieces : pieces + 2]
-        copies = [pltpu.make_async_copy(rest[k], rest[pieces + 2 + k], rest[-1].at[k]) for k in range(pieces)]
+        out_ref = rest[pieces]
+        copies = [pltpu.make_async_copy(rest[k], rest[pieces + 1 + k], rest[-1].at[k]) for k in range(pieces)]
         for copy in copies:
             copy.start()
-        rows_of = rows_for(where_ref, parts, tile)
+        rows_of = rows_for(where_ref, (0,), tile)
 
         def scores_at(h):
             query = rows_of(q_ref, slice(h * HD, (h + 1) * HD))
@@ -402,75 +410,57 @@
             if h + 1 < heads:
                 later = scores_at(h + 1)
             cols = slice(h * HD, (h + 1) * HD)
-            result = finished(scores, values_ref[h], rows_of(own_ref, cols), rows_of(log_ref)[:, h : h + 1])
-            out_a[:, cols] = result[:tile]
-            out_b[:, cols] = result[tile:]
+            out_ref[:, cols] = finished(
+                scores, values_ref[h], rows_of(own_ref, cols), rows_of(log_ref)[:, h : h + 1]
+            )
         for copy in copies:
             copy.wait()
 
     return pl.pallas_call(
         body,
         in_specs=[SMEM] + [VMEM] * 6 + [HBM] * pieces,
-        out_specs=[VMEM] * (2 + pieces),
-        out_shape=[in_vmem((tile, width), jnp.bfloat16)] * 2 + [in_vmem(w.shape, w.dtype) for w in carried],
+        out_specs=[VMEM] * (1 + pieces),
+        out_shape=[in_vmem((tile, width), jnp.bfloat16)] + [in_vmem(w.shape, w.dtype) for w in carried],
         scratch_shapes=[pltpu.SemaphoreType.DMA((pieces,))],
         compiler_params=params(),
-        cost_estimate=cost(4 * rows * count * width, 4 * count * width, rows * count * heads),
+        cost_estimate=cost(2 * rows * count * width, 4 * count * width, rows * count * heads),
         name="attend_second",
     )(where, query, keys, values, mask, own, log, *keep_in_hbm(*carried))
 
 
-def mix_near(core, attended, w_own, mine, other):
-    rows = attended[0].shape[0]
+def mix(core, attended, w_own, mine, other):
+    rows, width = attended[0].shape
     part = mine[0].shape[1]
 
-    def body(core_ref, own_ref, right_ref, far_ref, w_ref, *rest):
-        out_ref = rest[-1]
-        for side, pieces in enumerate((rest[:4], rest[4:8])):
+    def body(core_ref, *rest):
+        own_ref, far_refs, w_ref, pieces = rest[0], rest[1:4], rest[4], (rest[5:11], rest[11:17])
+        out_hbm, out_ref, sems = rest[17:]
+        copies = []
+        for side in range(2):
             base = (core_ref[0] if side == 0 else 1 - core_ref[0]) * 2
             for k in range(2):
                 span = pl.ds(pl.multiple_of((base + k) * part, part), part)
-                total = f32dot(own_ref[...], w_ref[:, span]) + f32dot(right_ref[...], pieces[k][...])
-                out_ref[:, span] = total + f32dot(far_ref[...], pieces[2 + k][...])
-
-    args = (*attended, w_own, *mine, *other)
-    return pl.pallas_call(
-        body,
-        in_specs=[SMEM] + [VMEM] * len(args),
-        out_specs=VMEM,
-        out_shape=in_vmem((rows, 4 * part), jnp.float32),
-        compiler_params=params(),
-        cost_estimate=cost(24 * rows * w_own.shape[0] * part, 24 * w_own.shape[0] * part),
-        name="mix_near",
-    )(core, *args)
-
-
-def mix_last(core, left, mine, other, before):
-    rows = left.shape[0]
-    part = mine[0].shape[1]
-
-    def body(core_ref, left_ref, *rest):
-        before_ref, out_hbm, out_ref, sems = rest[4:]
-        copies = []
-        for at in range(4):
-            base = (core_ref[0] if at < 2 else 1 - core_ref[0]) * 2
-            span = pl.ds(pl.multiple_of((base + at % 2) * part, part), part)
-            out_ref[at] = (before_ref[:, span] + f32dot(left_ref[...], rest[at][...])).astype(jnp.bfloat16)
-            copies.append(pltpu.make_async_copy(out_ref.at[at], out_hbm.at[:, span], sems.at[at]))
-            copies[-1].start()
+                total = f32dot(own_ref[...], w_ref[:, span])
+                for g in range(3):
+                    total = total + f32dot(far_refs[g][...], pieces[side][2 * g + k][...])
+                at = 2 * side + k
+                out_ref[at] = total.astype(jnp.bfloat16)
+                copies.append(pltpu.make_async_copy(out_ref.at[at], out_hbm.at[:, span], sems.at[at]))
+                copies[-1].start()
         for copy in copies:
             copy.wait()
 
-    return pl.pallas_call(
-        body,
-        in_specs=[SMEM] + [VMEM] * 6,
+    args = (*attended, w_own, *mine, *other)
+    return pl.pallas_call(
+        body,
+        in_specs=[SMEM] + [VMEM] * len(args),
         out_specs=HBM,
         out_shape=in_hbm((rows, 4 * part), jnp.bfloat16),
         scratch_shapes=[pltpu.VMEM((4, rows, part), jnp.bfloat16), pltpu.SemaphoreType.DMA((4,))],
         compiler_params=params(),
-        cost_estimate=cost(8 * rows * left.shape[1] * part, 8 * left.shape[1] * part),
-        name="mix_last",
-    )(core, left, *mine, *other, before)
+        cost_estimate=cost(32 * rows * width * part, 32 * width * part),
+        name="mix",
+    )(core, *args)
 
 
 def local(tokens, w_query, w_key, w_value, w_out, chosen):
@@ -511,17 +501,15 @@
 
     query = project_query(where, tokens, left, right, top, bottom, w_query)
     own, log = attend_own(query, pair, mask, peers * MOST)
-    to_far, to_left, keys, values, mask, own, log = attend_first(
-        where, query, got.reshape(-1, 2 * width), mask, own, log, (3, 1)
+    to_far, to_left, to_right, keys, values, mask, own, log = attend_first(
+        where, query, got.reshape(-1, 2 * width), mask, own, log, ((3, 1), (2,))
     )
     far = shifted(to_far, "tp", 2)
     right = shifted(to_left, "tp", -1)
+    left = shifted(to_right, "tp", 1)
     carried = (w_out, *mine, *other)
-    to_right, mid, w_own, *pieces = attend_second(where, query, keys, values, mask, own, log, (2, 0), carried)
-    left = shifted(to_right, "tp", 1)
-    mine, other = pieces[:6], pieces[6:]
-    before = mix_near(core, (mid, right, far), w_own, mine[2:], other[2:])
-    return mix_last(core, left, mine[:2], other[:2], before)
+    mid, w_own, *pieces = attend_second(where, query, keys, values, mask, own, log, carried)
+    return mix(core, (mid, left, right, far), w_own, pieces[:6], pieces[6:])
 
 
 def solution(mesh):

time: 109 us -> 107 us (0.982)
  waiting for transfers between devices: 44.1 us -> 41 us
  Pallas kernels: 29.6 us -> 30.7 us
    ppermute x19, waiting for transfers between devices: 40.6 us -> 37.6 us  [shifted(): lax.ppermute(array, axis, [(i, (i + by) % count) for i in range(count)])]
    pallas_call x1, Pallas kernels: 4.58 us -> 6.33 us  [attend_first(): pl.pallas_call(body, in_specs=[SMEM, VMEM, VMEM, HBM, HBM, HBM], out_spec...]
where the time goes in v3:
time: 107 us
  waiting for transfers between devices  41 us (38%)
  starting transfers between devices  31.2 us (29%)
  Pallas kernels  30.7 us (29%)
  local copies, waits for them, and re-layouts  3.67 us (3%)
    ppermute x19, waiting for transfers between devices, shifted(): lax.ppermute(array, axis, [(i, (i + by) % count) for i in range(count)])  37.6 us
    ppermute x19, starting transfers between devices, shifted(): lax.ppermute(array, axis, [(i, (i + by) % count) for i in range(count)])  16.6 us
    all_to_all x1, starting transfers between devices, local(): asked = lax.all_to_all(request, KV, 0, 0, tiled=True)  8.33 us
    pallas_call x1, Pallas kernels, attend_first(): pl.pallas_call(body, in_specs=[SMEM, VMEM, VMEM, HBM, HBM, HBM], out_spec...  6.33 us
    all_to_all x1, starting transfers between devices, local(): got = lax.all_to_all(send, KV, split_axis=0, concat_axis=0, tiled=True)  6.27 us
    pallas_call x1, Pallas kernels, attend_second(): pl.pallas_call(body, in_specs=[SMEM] + [VMEM] * 6 + [HBM] * pieces, out_s...  4.68 us
    pallas_call x1, Pallas kernels, project_near(): pl.pallas_call(body, in_specs=[SMEM, SMEM, HBM, VMEM, VMEM, HBM, HBM, HBM...  4.59 us
    pallas_call x1, Pallas kernels, attend_own(): pl.pallas_call(body, grid=(heads,), in_specs=[column, column, pl.BlockSpe...  4.57 us
  transfers between devices with their start and end apart: 21, of which 11 were waited for; matrix products, arithmetic and copies ran while one was open for 0% of the time, Pallas kernels for 23%

profile of v3, /device:TPU:0, one launch (start us, length us, event | category | flops | bytes accessed | tf_op | source)
XLA Modules:
  0.0 107.0 jit_solution(4270154515326888268)
XLA Ops:
  0.1 2.9 %collective-permute-start.1 = (bf16[512,512]{1,0:T(8,128)(2,1)}, bf16[512,512]{1,0:T(8,128)(2,1)S(1)}, u32[]{:S(2)}, u32[]{:S(2)}) collective-permute-start(bf16[512,512]{1,0:T(8,128)(2,1)} %o_ref), channel_id=1, source_target_pairs={{0,3},{1,0},{2,1},{3,2},{4,7},{5,4},{6,5},{7,6},{8,11},{9,8},{10,9... | collective-permute-start | bytes 1572872 | tf_op jit(solution)/shard_map/ppermute | solution.py:49
  3.0 0.7 copy-done
  3.7 1.0 plan.1
  4.6 9.8 %collective-permute-done.1.r_ref = bf16[512,512]{1,0:T(8,128)(2,1)S(1)} collective-permute-done((bf16[512,512]{1,0:T(8,128)(2,1)}, bf16[512,512]{1,0:T(8,128)(2,1)S(1)}, u32[]{:S(2)}, u32[]{:S(2)}) %collective-permute-start.1) | collective-permute-done | bytes 524320 | tf_op jit(solution)/shard_map/ppermute | solution.py:49
  14.5 3.3 %collective-permute-done.l_ref = bf16[512,512]{1,0:T(8,128)(2,1)S(1)} collective-permute-done((bf16[512,512]{1,0:T(8,128)(2,1)}, bf16[512,512]{1,0:T(8,128)(2,1)S(1)}, u32[]{:S(2)}, u32[]{:S(2)}) %collective-permute-start) | collective-permute-done | bytes 524320 | tf_op jit(solution)/shard_map/ppermute | solution.py:49
  17.8 0.7 slice.6
  18.5 0.7 slice.7
  19.5 1.7 %collective-permute-start.2 = (bf16[256,512]{1,0:T(8,128)(2,1)}, bf16[256,512]{1,0:T(8,128)(2,1)}, u32[]{:S(2)}, u32[]{:S(2)}) collective-permute-start(bf16[256,512]{1,0:T(8,128)(2,1)} %slice.6), channel_id=1, source_target_pairs={{0,1},{1,2},{2,3},{3,0},{4,5},{5,6},{6,7},{7,4},{8,9},{9,10},{10,1... | collective-permute-start | bytes 786440 | tf_op jit(solution)/shard_map/ppermute | solution.py:49
  21.2 8.3 %all-to-all-start = ((s32[32,1,128]{2,1,0:T(1,128)}), s32[32,1,128]{2,1,0:T(1,128)S(1)}, u32[]{:S(2)}, u32[]{:S(2)}) async-start(s32[32,1,128]{2,1,0:T(1,128)} %bitcast.13), calls=%async_computation | async-start | bytes 32768 | tf_op jit(solution)/shard_map/all_to_all | solution.py:481
  29.6 4.6 %project_near.1 = (f32[512,768]{1,0:T(8,128)S(1)}, bf16[512,384]{1,0:T(8,128)(2,1)S(1)}, bf16[512,384]{1,0:T(8,128)(2,1)S(1)}, bf16[512,512]{1,0:T(8,128)(2,1)},...) custom-call(s32[4]{0:T(128)S(1)} %pad_add_fusion.where_ref, ...), custom_call_target="tpu_custom_call" | custom-call | flops 1207959552 | bytes 3932160 | tf_op jit(solution)/shard_map/project_near/pallas_call | solution.py:89
  34.2 0.7 copy-done.1
  34.9 0.8 copy-done.3
  35.7 1.3 %all-to-all-done = s32[32,1,128]{2,1,0:T(1,128)S(1)} async-done(((s32[32,1,128]{2,1,0:T(1,128)}), s32[32,1,128]{2,1,0:T(1,128)S(1)}, u32[]{:S(2)}, u32[]{:S(2)}) %all-to-all-start) | async-done | bytes 16416 | tf_op jit(solution)/shard_map/all_to_all | solution.py:481
  37.0 3.8 %project_last.1 = (bf16[512,768]{1,0:T(8,128)(2,1)}, bf16[64,32,768]{2,1,0:T(8,128)(2,1)}, bf16[256,512]{1,0:T(8,128)(2,1)}, bf16[256,512]{1,0:T(8,128)(2,1)}) custom-call(s32[32,128]{1,0:T(8,128)S(1)} %bitcast.12, bf16[256,512]{1,0:T(8,128)(2,1)} %collective-permute-done.2.t_ref, bf16[256,512]{1,0:T(8,128)(2,1)} %collective-permute-done.3.b_ref, ...), custom_call_target="tpu_custom_call" | custom-call | flops 402653184 | bytes 2359296 | tf_op jit(solution)/shard_map/project_last/pallas_call | solution.py:149
  40.8 6.3 %all-to-all-start.1 = ((bf16[64,32,768]{2,1,0:T(8,128)(2,1)}), bf16[64,32,768]{2,1,0:T(8,128)(2,1)S(1)}, u32[]{:S(2)}, u32[]{:S(2)}) async-start(bf16[64,32,768]{2,1,0:T(8,128)(2,1)} %get-tuple-element.70), calls=%async_computation.1 | async-start | bytes 6291456 | tf_op jit(solution)/shard_map/all_to_all | solution.py:491
  47.1 1.6 %collective-permute-start.6 = (bf16[384,512]{1,0:T(8,128)(2,1)}, bf16[384,512]{1,0:T(8,128)(2,1)S(1)}, u32[]{:S(2)}, u32[]{:S(2)}) collective-permute-start(bf16[384,512]{1,0:T(8,128)(2,1)} %copy-done.3), channel_id=1, source_target_pairs={{0,3},{1,0},{2,1},{3,2},{4,7},{5,4},{6,5},{7,6},{8,11},{9,8},{10,9... | collective-permute-start | bytes 1179656 | tf_op jit(solution)/shard_map/ppermute | solution.py:49
  48.7 0.5 collective-permute-start.4
  49.2 2.7 %collective-permute-start.7 = (bf16[384,512]{1,0:T(8,128)(2,1)S(1)}, bf16[384,512]{1,0:T(8,128)(2,1)}, u32[]{:S(2)}, u32[]{:S(2)}) collective-permute-start(bf16[384,512]{1,0:T(8,128)(2,1)S(1)} %copy-done.2), channel_id=1, source_target_pairs={{0,3},{1,0},{2,1},{3,2},{4,7},{5,4},{6,5},{7,6},{8,11},{9,8},{10,9... | collective-permute-start | bytes 1179656 | tf_op jit(solution)/shard_map/ppermute | solution.py:49
  51.9 7.5 %collective-permute-done.6.rest_3_ = bf16[384,512]{1,0:T(8,128)(2,1)S(1)} collective-permute-done((bf16[384,512]{1,0:T(8,128)(2,1)}, bf16[384,512]{1,0:T(8,128)(2,1)S(1)}, u32[]{:S(2)}, u32[]{:S(2)}) %collective-permute-start.6) | collective-permute-done | bytes 393248 | tf_op jit(solution)/shard_map/ppermute | solution.py:49
  59.4 2.8 %collective-permute-done.4.rest_1_ = bf16[384,512]{1,0:T(8,128)(2,1)} collective-permute-done((bf16[384,512]{1,0:T(8,128)(2,1)}, bf16[384,512]{1,0:T(8,128)(2,1)}, u32[]{:S(2)}, u32[]{:S(2)}) %collective-permute-start.4) | collective-permute-done | bytes 393248 | tf_op jit(solution)/shard_map/ppermute | solution.py:49
  62.2 5.0 %collective-permute-done.7.rest_4_ = bf16[384,512]{1,0:T(8,128)(2,1)} collective-permute-done((bf16[384,512]{1,0:T(8,128)(2,1)S(1)}, bf16[384,512]{1,0:T(8,128)(2,1)}, u32[]{:S(2)}, u32[]{:S(2)}) %collective-permute-start.7) | collective-permute-done | bytes 393248 | tf_op jit(solution)/shard_map/ppermute | solution.py:49
  67.2 2.7 %collective-permute-start.9 = (bf16[384,512]{1,0:T(8,128)(2,1)}, bf16[384,512]{1,0:T(8,128)(2,1)}, u32[]{:S(2)}, u32[]{:S(2)}) collective-permute-start(bf16[384,512]{1,0:T(8,128)(2,1)} %collective-permute-done.7.rest_4_), channel_id=1, source_target_pairs={{0,3},{1,0},{2,1},{3,2},{4,7},{5,4},{6,5},{7,6},{8,11},{9,8},{10,9... | collective-permute-start | bytes 1179656 | tf_op jit(solution)/shard_map/ppermute | solution.py:49
  69.9 0.7 collective-permute-done.5.rest_2_
  71.1 6.9 %collective-permute-done.8.rest_5_ = bf16[384,512]{1,0:T(8,128)(2,1)} collective-permute-done((bf16[384,512]{1,0:T(8,128)(2,1)}, bf16[384,512]{1,0:T(8,128)(2,1)}, u32[]{:S(2)}, u32[]{:S(2)}) %collective-permute-start.8) | collective-permute-done | bytes 393248 | tf_op jit(solution)/shard_map/ppermute | solution.py:49
  78.6 3.8 %project_query.1.q_ref = bf16[512,384]{1,0:T(8,128)(2,1)S(1)} custom-call(s32[4]{0:T(128)S(1)} %pad_add_fusion.where_ref, bf16[512,512]{1,0:T(8,128)(2,1)} %o_ref, bf16[512,512]{1,0:T(8,128)(2,1)} %get-tuple-element.60.l_ref, bf16[512,512]{1,0:T(8,128)(2,1)} %get-tuple-element.61.r_ref, bf16[256,512]{1,0:T(8,128)(2,1)} %get-tuple-element.65.t_ref, ...), custom_call_target="tpu_custom_call" | custom-call | flops 805306368 | bytes 3145728 | tf_op jit(solution)/shard_map/project_query/pallas_call | solution.py:189
  82.3 4.6 %attend_own.1 = (f32[512,384]{1,0:T(8,128)}, f32[512,128]{1,0:T(8,128)}) custom-call(bf16[512,384]{1,0:T(8,128)(2,1)S(1)} %project_query.1.q_ref, bf16[512,768]{1,0:T(8,128)(2,1)} %get-tuple-element.72.k_ref.v_ref, bf16[512,768]{1,0:T(8,128)(2,1)} %get-tuple-element.72.k_ref.v_ref, bf16[512,128]{1,0:T(8,128)(2,1)} %get-tuple-element.71.mask_ref.mask_hbm), custom_call_target="tpu_custom_call" | custom-call | flops 805306368 | bytes 3145728 | tf_op jit(solution)/shard_map/attend_own/pallas_call | solution.py:296
  86.9 2.2 %all-to-all-done.1 = bf16[64,32,768]{2,1,0:T(8,128)(2,1)S(1)} async-done(((bf16[64,32,768]{2,1,0:T(8,128)(2,1)}), bf16[64,32,768]{2,1,0:T(8,128)(2,1)S(1)}, u32[]{:S(2)}, u32[]{:S(2)}) %all-to-all-start.1) | async-done | bytes 3145760 | tf_op jit(solution)/shard_map/all_to_all | solution.py:491
  89.1 6.3 %attend_first.1 = (bf16[128,384]{1,0:T(8,128)(2,1)S(1)}, bf16[128,384]{1,0:T(8,128)(2,1)S(1)}, bf16[128,384]{1,0:T(8,128)(2,1)S(1)}, bf16[3,2048,256]{2,1,0:T(8,...) custom-call(s32[4]{0:T(128)S(1)} %pad_add_fusion.where_ref, ...), custom_call_target="tpu_custom_call" | custom-call | flops 2415919104 | bytes 3145728 | tf_op jit(solution)/shard_map/attend_first/pallas_call | solution.py:372
  95.5 3.2 %collective-permute-start.17 = (bf16[128,384]{1,0:T(8,128)(2,1)S(1)}, bf16[128,384]{1,0:T(8,128)(2,1)S(1)}, u32[]{:S(2)}, u32[]{:S(2)}) collective-permute-start(bf16[128,384]{1,0:T(8,128)(2,1)S(1)} %get-tuple-element.84), channel_id=1, source_target_pairs={{0,3},{1,0},{2,1},{3,2},{4,7},{5,4},{6,5},{7,6},{8,11},{9,8},{10,9... | collective-permute-start | bytes 294920 | tf_op jit(solution)/shard_map/ppermute | solution.py:49
  98.8 4.7 %attend_second.1 = (bf16[128,384]{1,0:T(8,128)(2,1)S(1)}, bf16[384,2048]{1,0:T(8,128)(2,1)S(1)}, bf16[384,512]{1,0:T(8,128)(2,1)S(1)}, bf16[384,512]{1,0:T(8,128...) custom-call(s32[4]{0:T(128)S(1)} %pad_add_fusion.where_ref, ...), custom_call_target="tpu_custom_call" | custom-call | flops 805306368 | bytes 3145728 | tf_op jit(solution)/shard_map/attend_second/pallas_call | solution.py:419
  103.5 1.4 %collective-permute-done.18.rest_3_ = bf16[128,384]{1,0:T(8,128)(2,1)S(1)} collective-permute-done((bf16[128,384]{1,0:T(8,128)(2,1)S(1)}, bf16[128,384]{1,0:T(8,128)(2,1)S(1)}, u32[]{:S(2)}, u32[]{:S(2)}) %collective-permute-start.18) | collective-permute-done | bytes 98336 | tf_op jit(solution)/shard_map/ppermute | solution.py:49
  104.9 2.0 %mix.1 = bf16[128,2048]{1,0:T(8,128)(2,1)} custom-call(s32[1]{0:T(128)} %bitcast.5.core_ref, bf16[128,384]{1,0:T(8,128)(2,1)S(1)} %get-tuple-element.82.rest_0_, bf16[128,384]{1,0:T(8,128)(2,1)S(1)} %collective-permute-done.16.rest_1_, bf16[128,384]{1,0:T(8,128)(2,1)S(1)} %collective-permute-done.17.rest_2_, ...), custom_call_target="tpu_custom_call" | custom-call | flops 805306368 | bytes 6291456 | tf_op jit(solution)/shard_map/mix/pallas_call | solution.py:454
  (33 shorter events, 1.5 us)
Async XLA Ops:
  0.1 14.4 %collective-permute-start.1 = (bf16[512,512]{1,0:T(8,128)(2,1)}, bf16[512,512]{1,0:T(8,128)(2,1)S(1)}, u32[]{:S(2)}, u32[]{:S(2)}) collective-permute-start(bf16[512,512]{1,0:T(8,128)(2,1)} %o_ref), channel_id=1, source_target_pairs={{0,3},{1,0},{2,1},{3,2},{4,7},{5,4},{6,5},{7,6},{8,11},{9,8},{10,9... | collective-permute-start | bytes 1572872 | tf_op jit(solution)/shard_map/ppermute | solution.py:49
  3.0 14.8 %collective-permute-start = (bf16[512,512]{1,0:T(8,128)(2,1)}, bf16[512,512]{1,0:T(8,128)(2,1)S(1)}, u32[]{:S(2)}, u32[]{:S(2)}) collective-permute-start(bf16[512,512]{1,0:T(8,128)(2,1)} %o_ref), channel_id=1, source_target_pairs={{0,1},{1,2},{2,3},{3,0},{4,5},{5,6},{6,7},{7,4},{8,9},{9,10},{10,1... | collective-permute-start | bytes 1572872 | tf_op jit(solution)/shard_map/ppermute | solution.py:49
  3.0 0.7 copy-start
  19.2 17.7 %collective-permute-start.3 = (bf16[256,512]{1,0:T(8,128)(2,1)}, bf16[256,512]{1,0:T(8,128)(2,1)}, u32[]{:S(2)}, u32[]{:S(2)}) collective-permute-start(bf16[256,512]{1,0:T(8,128)(2,1)} %slice.7), channel_id=1, source_target_pairs={{0,3},{1,0},{2,1},{3,2},{4,7},{5,4},{6,5},{7,6},{8,11},{9,8},{10,9... | collective-permute-start | bytes 786440 | tf_op jit(solution)/shard_map/ppermute | solution.py:49
  19.5 17.5 %collective-permute-start.2 = (bf16[256,512]{1,0:T(8,128)(2,1)}, bf16[256,512]{1,0:T(8,128)(2,1)}, u32[]{:S(2)}, u32[]{:S(2)}) collective-permute-start(bf16[256,512]{1,0:T(8,128)(2,1)} %slice.6), channel_id=1, source_target_pairs={{0,1},{1,2},{2,3},{3,0},{4,5},{5,6},{6,7},{7,4},{8,9},{9,10},{10,1... | collective-permute-start | bytes 786440 | tf_op jit(solution)/shard_map/ppermute | solution.py:49
  21.2 15.7 %all-to-all-start = ((s32[32,1,128]{2,1,0:T(1,128)}), s32[32,1,128]{2,1,0:T(1,128)S(1)}, u32[]{:S(2)}, u32[]{:S(2)}) async-start(s32[32,1,128]{2,1,0:T(1,128)} %bitcast.13), calls=%async_computation | async-start | bytes 32768 | tf_op jit(solution)/shard_map/all_to_all | solution.py:481
  34.2 0.8 copy-start.1
  34.9 0.8 copy-start.3
  40.8 8.4 %copy-start.2 = (bf16[384,512]{1,0:T(8,128)(2,1)S(1)}, bf16[384,512]{1,0:T(8,128)(2,1)}, u32[]{:S(2)}) copy-start(bf16[384,512]{1,0:T(8,128)(2,1)} %copy-done.1) | copy-start | bytes 1179652
  40.8 48.3 %all-to-all-start.1 = ((bf16[64,32,768]{2,1,0:T(8,128)(2,1)}), bf16[64,32,768]{2,1,0:T(8,128)(2,1)S(1)}, u32[]{:S(2)}, u32[]{:S(2)}) async-start(bf16[64,32,768]{2,1,0:T(8,128)(2,1)} %get-tuple-element.70), calls=%async_computation.1 | async-start | bytes 6291456 | tf_op jit(solution)/shard_map/all_to_all | solution.py:491
  47.1 12.3 %collective-permute-start.6 = (bf16[384,512]{1,0:T(8,128)(2,1)}, bf16[384,512]{1,0:T(8,128)(2,1)S(1)}, u32[]{:S(2)}, u32[]{:S(2)}) collective-permute-start(bf16[384,512]{1,0:T(8,128)(2,1)} %copy-done.3), channel_id=1, source_target_pairs={{0,3},{1,0},{2,1},{3,2},{4,7},{5,4},{6,5},{7,6},{8,11},{9,8},{10,9... | collective-permute-start | bytes 1179656 | tf_op jit(solution)/shard_map/ppermute | solution.py:49
  48.7 13.5 %collective-permute-start.4 = (bf16[384,512]{1,0:T(8,128)(2,1)}, bf16[384,512]{1,0:T(8,128)(2,1)}, u32[]{:S(2)}, u32[]{:S(2)}) collective-permute-start(bf16[384,512]{1,0:T(8,128)(2,1)} %copy-done.3), channel_id=1, source_target_pairs={{0,1},{1,2},{2,3},{3,0},{4,5},{5,6},{6,7},{7,4},{8,9},{9,10},{10,1... | collective-permute-start | bytes 1179656 | tf_op jit(solution)/shard_map/ppermute | solution.py:49
  49.2 18.0 %collective-permute-start.7 = (bf16[384,512]{1,0:T(8,128)(2,1)S(1)}, bf16[384,512]{1,0:T(8,128)(2,1)}, u32[]{:S(2)}, u32[]{:S(2)}) collective-permute-start(bf16[384,512]{1,0:T(8,128)(2,1)S(1)} %copy-done.2), channel_id=1, source_target_pairs={{0,3},{1,0},{2,1},{3,2},{4,7},{5,4},{6,5},{7,6},{8,11},{9,8},{10,9... | collective-permute-start | bytes 1179656 | tf_op jit(solution)/shard_map/ppermute | solution.py:49
  51.9 18.7 %collective-permute-start.5 = (bf16[384,512]{1,0:T(8,128)(2,1)S(1)}, bf16[384,512]{1,0:T(8,128)(2,1)}, u32[]{:S(2)}, u32[]{:S(2)}) collective-permute-start(bf16[384,512]{1,0:T(8,128)(2,1)S(1)} %copy-done.2), channel_id=1, source_target_pairs={{0,1},{1,2},{2,3},{3,0},{4,5},{5,6},{6,7},{7,4},{8,9},{9,10},{10,1... | collective-permute-start | bytes 1179656 | tf_op jit(solution)/shard_map/ppermute | solution.py:49
  59.4 19.2 %copy-start.4 = (bf16[384,512]{1,0:T(8,128)(2,1)}, bf16[384,512]{1,0:T(8,128)(2,1)S(1)}, u32[]{:S(2)}) copy-start(bf16[384,512]{1,0:T(8,128)(2,1)S(1)} %collective-permute-done.6.rest_3_) | copy-start | bytes 1179652
  59.4 11.2 %collective-permute-start.12 = (bf16[384,512]{1,0:T(8,128)(2,1)S(1)}, bf16[384,512]{1,0:T(8,128)(2,1)S(1)}, u32[]{:S(2)}, u32[]{:S(2)}) collective-permute-start(bf16[384,512]{1,0:T(8,128)(2,1)S(1)} %collective-permute-done.6.rest_3_), channel_id=1, source_target_pairs={{0,4},{4,0},{1,5},{5,1},{2,6},{6,2},{3,7},{7,3},{8,12},{12,8},{9,1... | collective-permute-start | bytes 1179656 | tf_op jit(solution)/shard_map/ppermute | solution.py:49
  62.2 15.9 %collective-permute-start.8 = (bf16[384,512]{1,0:T(8,128)(2,1)}, bf16[384,512]{1,0:T(8,128)(2,1)}, u32[]{:S(2)}, u32[]{:S(2)}) collective-permute-start(bf16[384,512]{1,0:T(8,128)(2,1)} %collective-permute-done.4.rest_1_), channel_id=1, source_target_pairs={{0,1},{1,2},{2,3},{3,0},{4,5},{5,6},{6,7},{7,4},{8,9},{9,10},{10,1... | collective-permute-start | bytes 1179656 | tf_op jit(solution)/shard_map/ppermute | solution.py:49
  67.2 11.0 %collective-permute-start.9 = (bf16[384,512]{1,0:T(8,128)(2,1)}, bf16[384,512]{1,0:T(8,128)(2,1)}, u32[]{:S(2)}, u32[]{:S(2)}) collective-permute-start(bf16[384,512]{1,0:T(8,128)(2,1)} %collective-permute-done.7.rest_4_), channel_id=1, source_target_pairs={{0,3},{1,0},{2,1},{3,2},{4,7},{5,4},{6,5},{7,6},{8,11},{9,8},{10,9... | collective-permute-start | bytes 1179656 | tf_op jit(solution)/shard_map/ppermute | solution.py:49
  69.9 25.5 %collective-permute-start.10 = (bf16[384,512]{1,0:T(8,128)(2,1)}, bf16[384,512]{1,0:T(8,128)(2,1)}, u32[]{:S(2)}, u32[]{:S(2)}) collective-permute-start(bf16[384,512]{1,0:T(8,128)(2,1)} %collective-permute-done.4.rest_1_), channel_id=1, source_target_pairs={{0,4},{4,0},{1,5},{5,1},{2,6},{6,2},{3,7},{7,3},{8,12},{12,8},{9,1... | collective-permute-start | bytes 1179656 | tf_op jit(solution)/shard_map/ppermute | solution.py:49
  70.6 24.9 %collective-permute-start.13 = (bf16[384,512]{1,0:T(8,128)(2,1)}, bf16[384,512]{1,0:T(8,128)(2,1)}, u32[]{:S(2)}, u32[]{:S(2)}) collective-permute-start(bf16[384,512]{1,0:T(8,128)(2,1)} %collective-permute-done.7.rest_4_), channel_id=1, source_target_pairs={{0,4},{4,0},{1,5},{5,1},{2,6},{6,2},{3,7},{7,3},{8,12},{12,8},{9,1... | collective-permute-start | bytes 1179656 | tf_op jit(solution)/shard_map/ppermute | solution.py:49
  70.6 8.0 %copy-start.5 = (bf16[384,512]{1,0:T(8,128)(2,1)}, bf16[384,512]{1,0:T(8,128)(2,1)S(1)}, u32[]{:S(2)}) copy-start(bf16[384,512]{1,0:T(8,128)(2,1)S(1)} %collective-permute-done.12.rest_9_) | copy-start | bytes 1179652
  70.6 28.2 %collective-permute-start.11 = (bf16[384,512]{1,0:T(8,128)(2,1)}, bf16[384,512]{1,0:T(8,128)(2,1)}, u32[]{:S(2)}, u32[]{:S(2)}) collective-permute-start(bf16[384,512]{1,0:T(8,128)(2,1)} %collective-permute-done.5.rest_2_), channel_id=1, source_target_pairs={{0,4},{4,0},{1,5},{5,1},{2,6},{6,2},{3,7},{7,3},{8,12},{12,8},{9,1... | collective-permute-start | bytes 1179656 | tf_op jit(solution)/shard_map/ppermute | solution.py:49
  78.1 20.7 %collective-permute-start.14 = (bf16[384,512]{1,0:T(8,128)(2,1)}, bf16[384,512]{1,0:T(8,128)(2,1)}, u32[]{:S(2)}, u32[]{:S(2)}) collective-permute-start(bf16[384,512]{1,0:T(8,128)(2,1)} %collective-permute-done.8.rest_5_), channel_id=1, source_target_pairs={{0,4},{4,0},{1,5},{5,1},{2,6},{6,2},{3,7},{7,3},{8,12},{12,8},{9,1... | collective-permute-start | bytes 1179656 | tf_op jit(solution)/shard_map/ppermute | solution.py:49
  78.2 20.6 %collective-permute-start.15 = (bf16[384,512]{1,0:T(8,128)(2,1)}, bf16[384,512]{1,0:T(8,128)(2,1)}, u32[]{:S(2)}, u32[]{:S(2)}) collective-permute-start(bf16[384,512]{1,0:T(8,128)(2,1)} %collective-permute-done.9.rest_6_), channel_id=1, source_target_pairs={{0,4},{4,0},{1,5},{5,1},{2,6},{6,2},{3,7},{7,3},{8,12},{12,8},{9,1... | collective-permute-start | bytes 1179656 | tf_op jit(solution)/shard_map/ppermute | solution.py:49
  95.5 8.0 %collective-permute-start.16 = (bf16[128,384]{1,0:T(8,128)(2,1)S(1)}, bf16[128,384]{1,0:T(8,128)(2,1)S(1)}, u32[]{:S(2)}, u32[]{:S(2)}) collective-permute-start(bf16[128,384]{1,0:T(8,128)(2,1)S(1)} %get-tuple-element.83), channel_id=1, source_target_pairs={{0,1},{1,2},{2,3},{3,0},{4,5},{5,6},{6,7},{7,4},{8,9},{9,10},{10,1... | collective-permute-start | bytes 294920 | tf_op jit(solution)/shard_map/ppermute | solution.py:49
  95.5 7.9 %collective-permute-start.17 = (bf16[128,384]{1,0:T(8,128)(2,1)S(1)}, bf16[128,384]{1,0:T(8,128)(2,1)S(1)}, u32[]{:S(2)}, u32[]{:S(2)}) collective-permute-start(bf16[128,384]{1,0:T(8,128)(2,1)S(1)} %get-tuple-element.84), channel_id=1, source_target_pairs={{0,3},{1,0},{2,1},{3,2},{4,7},{5,4},{6,5},{7,6},{8,11},{9,8},{10,9... | collective-permute-start | bytes 294920 | tf_op jit(solution)/shard_map/ppermute | solution.py:49
  98.8 6.1 %collective-permute-start.18 = (bf16[128,384]{1,0:T(8,128)(2,1)S(1)}, bf16[128,384]{1,0:T(8,128)(2,1)S(1)}, u32[]{:S(2)}, u32[]{:S(2)}) collective-permute-start(bf16[128,384]{1,0:T(8,128)(2,1)S(1)} %get-tuple-element.85), channel_id=1, source_target_pairs={{0,2},{1,3},{2,0},{3,1},{4,6},{5,7},{6,4},{7,5},{8,10},{9,11},{10,... | collective-permute-start | bytes 294920 | tf_op jit(solution)/shard_map/ppermute | solution.py:49
